TPU v7x, 32 devices: a whole 2x2x4 slice. The times are simulated.
32 devices in a mesh: sp: 8 (over z, x), tp: 4 (over y, core).
Axes of the slice: x: 2, y: 2, z: 4, core: 2. Of those that a mesh axis runs over, the one named last changes fastest.
Arguments:
- residual_in: bfloat16 [8192, 2048], P(('sp', 'tp')), may hold values from -6 to 6
- gate_outer: bfloat16 [8192, 1024], P('sp', 'tp'), may hold values from -6 to 6
- gate_inner: bfloat16 [8192, 1024], P('sp', 'tp'), may hold values from -6 to 6
- conv_input: bfloat16 [8192, 1024], P('sp', 'tp'), may hold values from -6 to 6
- conv_taps: bfloat16 [3, 1024], P(None, 'tp'), may hold values from -5 to 5
- norm_gain: bfloat16 [1024], P('tp'), may hold values from 0.099609375 to 1.8984375
- out_weight: bfloat16 [1024, 2048], P('tp'), may hold values from -0.1875 to 0.1875
- moe_gain: bfloat16 [2048], replicated, may hold values from 0.099609375 to 1.8984375
- expert_ids: int32 [8192, 2], P(('sp', 'tp')), may hold values from 0 to 7, all different within a row; in each aligned block of 256 rows (0 to 255, 256 to 511, ...) at most 128 rows name the same one
- group_prob: float32 [8192], P(('sp', 'tp')), may hold values from 0.3 to 1
- route_prob: float32 [8192, 2], P(('sp', 'tp')), may hold values from 0.1 to 1
- expert_gate: bfloat16 [8, 2048, 512], P('sp'), may hold values from -0.125 to 0.125
- expert_up: bfloat16 [8, 2048, 512], P('sp'), may hold values from -0.125 to 0.125
- expert_down: bfloat16 [8, 512, 2048], P('sp'), may hold values from -0.25 to 0.25
Outputs:
- layer_out: bfloat16 [8192, 2048], P(('sp', 'tp'))
Inputs may be any that keep to these rules, and one draw needn't show every extreme that they name: `expert_ids`: each row names 2 different experts. Within the rows of one device (aligned blocks of 256 rows) no expert is named more than 128 times.
All inputs are finite; a program needn't handle non-finite values.
Results may differ from a plain program's by a relative error of at most 0.0075.
Values may be sent and summed in bfloat16 or wider, within the bound.
A program may use at most 64 MiB of HBM per device.

v0:
```python
import jax
import jax.numpy as jnp
from jax import lax
from jax.sharding import PartitionSpec as P

EPSILON = 1e-06


def from_behind(shard, axis, by):
    devices = lax.axis_size(axis)
    pairs = [(i, i + by) for i in range(devices) if 0 <= i + by < devices]
    return lax.ppermute(shard, axis, pairs)


def rms_norm(values, gain):
    floats = values.astype(jnp.float32)
    factor = lax.rsqrt(jnp.mean(floats * floats, axis=-1, keepdims=True) + EPSILON)
    return floats * factor * gain.astype(jnp.float32)


def body(
    residual_in,
    gate_outer,
    gate_inner,
    conv_input,
    conv_taps,
    norm_gain,
    out_weight,
    moe_gain,
    expert_ids,
    group_prob,
    route_prob,
    expert_gate,
    expert_up,
    expert_down,
):
    seq_rows, channels = conv_input.shape
    taps_count = conv_taps.shape[0]
    inner = gate_inner.astype(jnp.float32) * conv_input.astype(jnp.float32)
    earlier = from_behind(inner[seq_rows - (taps_count - 1) :], "sp", 1)
    padded = jnp.concatenate([earlier, inner], axis=0)
    tap_f = conv_taps.astype(jnp.float32)
    filtered = jnp.zeros((seq_rows, channels), jnp.float32)
    for offset in range(taps_count):
        filtered = filtered + tap_f[offset][None, :] * padded[offset : offset + seq_rows]
    mixed_out = (gate_outer.astype(jnp.float32) * filtered).astype(jnp.bfloat16)
    gathered = lax.all_to_all(mixed_out, "tp", split_axis=0, concat_axis=1, tiled=True)
    full_weight, full_gain = (
        lax.all_gather(out_weight, "tp", axis=0, tiled=True),
        lax.all_gather(norm_gain, "tp", axis=0, tiled=True),
    )
    normed = rms_norm(gathered, full_gain).astype(jnp.bfloat16)
    projected = jnp.dot(normed, full_weight, preferred_element_type=jnp.float32)
    residual = (residual_in.astype(jnp.float32) + projected).astype(jnp.bfloat16)
    routed_in = rms_norm(residual, moe_gain).astype(jnp.bfloat16)
    tok_rows, width = routed_in.shape
    top_count = expert_ids.shape[1]
    local_count = expert_gate.shape[0]
    group_count = lax.axis_size("sp")
    experts_all = local_count * group_count
    capacity = 2 * tok_rows * top_count // experts_all
    slots = tok_rows * top_count
    flat_e = expert_ids.reshape(-1)
    one_hot = (flat_e[:, None] == jnp.arange(experts_all, dtype=jnp.int32)[None, :]).astype(
        jnp.int32
    )
    slot_rank = jnp.sum((jnp.cumsum(one_hot, axis=0) - 1) * one_hot, axis=1)
    owner_dev = flat_e // local_count
    local_slot = flat_e % local_count
    position = (local_slot * group_count + owner_dev) * capacity + slot_rank
    source_slot = (
        jnp.full((experts_all * capacity,), slots, jnp.int32)
        .at[position]
        .set(jnp.arange(slots, dtype=jnp.int32))
    )
    rows_pad = jnp.concatenate([routed_in, jnp.zeros((1, width), jnp.bfloat16)], axis=0)
    outgoing = rows_pad[source_slot // top_count].reshape(local_count, group_count, capacity, width)
    arrived = lax.all_to_all(outgoing, "sp", split_axis=1, concat_axis=1, tiled=True)
    gate_act = jnp.einsum(
        "esrd,edf->esrf", arrived, expert_gate, preferred_element_type=jnp.float32
    )
    up_act = jnp.einsum("esrd,edf->esrf", arrived, expert_up, preferred_element_type=jnp.float32)
    hidden = (jax.nn.silu(gate_act) * up_act).astype(jnp.bfloat16)
    result = jnp.einsum(
        "esrf,efd->esrd", hidden, expert_down, preferred_element_type=jnp.float32
    ).astype(jnp.bfloat16)
    returned = lax.all_to_all(result, "sp", split_axis=1, concat_axis=1, tiled=True)
    slot_out = returned.reshape(-1, width)[position].reshape(tok_rows, top_count, width)
    weights = group_prob[:, None] * route_prob / jnp.sum(route_prob, axis=1, keepdims=True)
    expert_sum = jnp.sum(slot_out.astype(jnp.float32) * weights[:, :, None], axis=1)
    return (residual.astype(jnp.float32) + expert_sum).astype(jnp.bfloat16)


def solution(mesh):
    in_specs = (
        P(("sp", "tp"), None),
        P("sp", "tp"),
        P("sp", "tp"),
        P("sp", "tp"),
        P(None, "tp"),
        P("tp"),
        P("tp", None),
        P(),
        P(("sp", "tp"), None),
        P(("sp", "tp")),
        P(("sp", "tp"), None),
        P("sp", None, None),
        P("sp", None, None),
        P("sp", None, None),
    )
    out_specs = P(("sp", "tp"), None)
    return jax.shard_map(body, mesh=mesh, in_specs=in_specs, out_specs=out_specs, check_vma=False)
```

profile of v0, /device:TPU:0, one launch (start us, length us, event | category | flops | bytes accessed | tf_op | source)
XLA Modules:
  0.0 305.5 jit_solution(6382998400257712995)
XLA Ops:
  6.6 0.7 all-gather.3.cloned.1.call-update
  7.3 1.3 convert_multiply_fusion.3
  8.6 4.9 %collective-permute-start = (f32[2,256]{1,0:T(2,128)S(1)}, f32[2,256]{1,0:T(2,128)S(1)}, u32[]{:S(2)}, u32[]{:S(2)}) collective-permute-start(f32[2,256]{1,0:T(2,128)S(1)} %slice.37), channel_id=1, source_target_pairs={{0,4},{4,8},{8,12},{12,16},{16,20},{20,24},{24,28},{1,5},{5,9},{9,... | collective-permute-start | bytes 6152 | tf_op jit(solution)/shard_map/ppermute | solution.py:12
  13.6 0.1 eq.31
  13.8 0.1 eq.27
  13.9 1.1 reduce-window.6
  15.1 0.2 slice_reduce_fusion
  15.5 5.1 %all-gather = bf16[4,1,256]{2,1,0:T(2,128)(2,1)S(1)} all-gather(bf16[1,1,256]{2,1,0:T(2,128)(2,1)S(1)} %reshape.144), channel_id=1, replica_groups=mesh['sp'=8,'tp'=4] {'tp'}, dimensions={0}, use_global_device_ids=true | all-gather | bytes 2560 | tf_op jit(solution)/shard_map/all_gather | solution.py:50
  20.7 0.1 mul.147
  20.9 2.3 fusion.25
  23.1 3.5 %all-to-all-start = ((bf16[4,256,256]{2,1,0:T(8,128)(2,1)}), bf16[4,256,256]{2,1,0:T(8,128)(2,1)S(1)}, u32[]{:S(2)}, u32[]{:S(2)}) async-start(bf16[4,256,256]{2,1,0:T(8,128)(2,1)} %bitcast.57), calls=%async_computation | async-start | bytes 1048576 | tf_op jit(solution)/shard_map/all_to_all | solution.py:47
  26.6 2.4 scatter_custom_fusion
  29.1 12.3 %all-to-all-done = bf16[4,256,256]{2,1,0:T(8,128)(2,1)S(1)} async-done(((bf16[4,256,256]{2,1,0:T(8,128)(2,1)}), bf16[4,256,256]{2,1,0:T(8,128)(2,1)S(1)}, u32[]{:S(2)}, u32[]{:S(2)}) %all-to-all-start) | async-done | bytes 524320 | tf_op jit(solution)/shard_map/all_to_all | solution.py:47
  41.4 1.1 convert_bitcast_fusion.1
  42.5 2.6 copy.25
  45.1 0.2 fusion.26
  45.3 1.5 fusion.29
  46.7 5.0 %all-gather.3.cloned.1.call-done = bf16[1024,2048]{1,0:T(8,128)(2,1)} async-done(((bf16[256,2048]{1,0:T(8,128)(2,1)}), bf16[1024,2048]{1,0:T(8,128)(2,1)}) %all-gather.3.cloned.1.call-update) | async-done | bytes 4194320 | tf_op jit(solution)/shard_map/all_gather | solution.py:49
  51.8 3.9 %fusion.5 = (f32[256]{0:T(256)S(1)}, bf16[256,2048]{1,0:T(8,128)(2,1)S(1)}) fusion(bf16[256,1024]{0,1:T(8,128)(2,1)S(1)} %fusion.29, bf16[1024,2048]{1,0:T(8,128)(2,1)} %all-gather.3.cloned.1.call-done, bf16[256,2048]{1,0:T(8,128)(2,1)} %param.14), kind=kOutput, calls=%fused_computation.14 | convolution fusion | flops 1076887296 | bytes 6816768 | tf_op jit(solution)/shard_map/dot_general | solution.py:53
  55.7 1.0 copy-done.2
  56.6 0.3 fusion.7
  57.0 6.0 %gather_fusion = bf16[1024,2048]{1,0:T(8,128)(2,1)} fusion(bf16[257,2048]{1,0:T(8,128)(2,1)S(1)} %concatenate.7, s32[1024]{0:T(1024)S(1)} %fusion.34), kind=kCustom, calls=%fused_computation | custom fusion | bytes 8392704 | tf_op jit(solution)/shard_map/gather | solution.py:77
  63.0 99.2 %all_to_all.23 = bf16[1,8,128,2048]{3,2,0,1:T(8,128)(2,1)S(1)} all-to-all(bf16[1,8,128,2048]{3,2,0,1:T(8,128)(2,1)} %bitcast.56), channel_id=1, replica_groups=mesh['sp'=8,'tp'=4] {'sp'}, dimensions={1} | all-to-all | bytes 8388608 | tf_op jit(solution)/shard_map/all_to_all | solution.py:78
  162.2 2.0 copy-done.1
  164.2 3.7 %fusion.2 = f32[8,128,512]{2,1,0:T(8,128)} fusion(bf16[1,8,128,2048]{3,2,0,1:T(8,128)(2,1)S(1)} %all_to_all.23, bf16[1,2048,512]{2,1,0:T(8,128)(2,1)S(1)} %copy-done.9), kind=kOutput, calls=%fused_computation.5 | convolution fusion | flops 2147483648 | bytes 8388608 | tf_op jit(solution)/shard_map/esrd,edf->esrf/dot_general | solution.py:79
  167.9 10.0 %convert_bitcast_fusion = bf16[1,8,128,2048]{3,2,0,1:T(8,128)(2,1)} fusion(bf16[1,512,2048]{2,1,0:T(8,128)(2,1)S(1)} %copy-done, f32[8,128,512]{2,1,0:T(8,128)} %fusion.2, bf16[1,2048,512]{2,1,0:T(8,128)(2,1)} %param.26, bf16[1,8,128,2048]{3,2,0,1:T(8,128)(2,1)} %copy-done.1), kind=kOutput, calls=%fused_computation.8 | convolution fusion | flops 4300210176 | bytes 14680064 | tf_op jit(solution)/shard_map/esrf,efd->esrd/dot_general | solution.py:84
  177.9 4.9 %all-to-all-start.2 = ((bf16[1,8,128,2048]{3,2,0,1:T(8,128)(2,1)}), bf16[1,8,128,2048]{3,2,0,1:T(8,128)(2,1)}, u32[]{:S(2)}, u32[]{:S(2)}) async-start(bf16[1,8,128,2048]{3,2,0,1:T(8,128)(2,1)} %convert_bitcast_fusion), calls=%async_computation.2 | async-start | bytes 8388608 | tf_op jit(solution)/shard_map/all_to_all | solution.py:87
  183.0 92.0 %all-to-all-done.2 = bf16[1,8,128,2048]{3,2,0,1:T(8,128)(2,1)} async-done(((bf16[1,8,128,2048]{3,2,0,1:T(8,128)(2,1)}), bf16[1,8,128,2048]{3,2,0,1:T(8,128)(2,1)}, u32[]{:S(2)}, u32[]{:S(2)}) %all-to-all-start.2) | async-done | bytes 4194336 | tf_op jit(solution)/shard_map/all_to_all | solution.py:87
  275.0 8.0 %gather_fusion.1 = bf16[512,2048]{1,0:T(8,128)(2,1)} fusion(bf16[1024,2048]{1,0:T(8,128)(2,1)} %bitcast.22, s32[1024]{0:T(1024)S(1)} %pad_clamp_fusion), kind=kCustom, calls=%fused_computation.1 | custom fusion | bytes 4196352 | tf_op jit(solution)/shard_map/gather | solution.py:88
  282.9 5.4 %reshape.118 = f32[256,2,2048]{2,1,0:T(2,128)} reshape(bf16[512,2048]{1,0:T(8,128)(2,1)} %gather_fusion.1) | data formatting | bytes 6291456 | tf_op jit(solution)/shard_map/convert_element_type | solution.py:90
  288.4 9.0 %multiply_reduce_fusion = f32[256,2048]{1,0:T(8,128)S(1)} fusion(f32[256,2,2048]{2,1,0:T(2,128)} %reshape.118, f32[256,2]{1,0:T(8,128)S(1)} %copy.31), kind=kLoop, calls=%fused_computation.7 | loop fusion | flops 1572864 | bytes 6293504 | tf_op jit(solution)/shard_map/reduce_sum | solution.py:90
  297.4 1.3 fusion.8
  (44 shorter events, 0.8 us)
Async XLA Ops:
  6.5 161.4 %copy-start = (bf16[1,512,2048]{2,1,0:T(8,128)(2,1)S(1)}, bf16[1,512,2048]{2,1,0:T(8,128)(2,1)}, u32[]{:S(2)}) copy-start(bf16[1,512,2048]{2,1,0:T(8,128)(2,1)} %param.27) | copy-start | bytes 6291460
  6.5 7.0 %copy-start.4 = (s32[256,2]{0,1:T(2,128)S(1)}, s32[256,2]{0,1:T(2,128)}, u32[]{:S(2)}) copy-start(s32[256,2]{0,1:T(2,128)} %param.22) | copy-start | bytes 6148
  6.5 8.8 %copy-start.6 = (bf16[3,256]{1,0:T(4,128)(2,1)S(1)}, bf16[3,256]{1,0:T(4,128)(2,1)}, u32[]{:S(2)}) copy-start(bf16[3,256]{1,0:T(4,128)(2,1)} %param.18) | copy-start | bytes 4612
  6.5 8.9 %copy-start.10 = (bf16[256]{0:T(256)(128)(2,1)S(1)}, bf16[256]{0:T(256)(128)(2,1)}, u32[]{:S(2)}) copy-start(bf16[256]{0:T(256)(128)(2,1)} %param.19) | copy-start | bytes 1540
  6.5 14.0 %copy-start.7 = (bf16[2048]{0:T(1024)(128)(2,1)S(1)}, bf16[2048]{0:T(1024)(128)(2,1)}, u32[]{:S(2)}) copy-start(bf16[2048]{0:T(1024)(128)(2,1)} %param.21) | copy-start | bytes 12292
  6.5 45.2 %all-gather.3.cloned.1.call-start = ((), (), s32[]{:S(2)}) async-start(), calls=%async_computation.3 | async-start | bytes 5242880 | tf_op jit(solution)/shard_map/all_gather | solution.py:49
  8.6 12.2 %collective-permute-start = (f32[2,256]{1,0:T(2,128)S(1)}, f32[2,256]{1,0:T(2,128)S(1)}, u32[]{:S(2)}, u32[]{:S(2)}) collective-permute-start(f32[2,256]{1,0:T(2,128)S(1)} %slice.37), channel_id=1, source_target_pairs={{0,4},{4,8},{8,12},{12,16},{16,20},{20,24},{24,28},{1,5},{5,9},{9,... | collective-permute-start | bytes 6152 | tf_op jit(solution)/shard_map/ppermute | solution.py:12
  23.1 18.3 %all-to-all-start = ((bf16[4,256,256]{2,1,0:T(8,128)(2,1)}), bf16[4,256,256]{2,1,0:T(8,128)(2,1)S(1)}, u32[]{:S(2)}, u32[]{:S(2)}) async-start(bf16[4,256,256]{2,1,0:T(8,128)(2,1)} %bitcast.57), calls=%async_computation | async-start | bytes 1048576 | tf_op jit(solution)/shard_map/all_to_all | solution.py:47
  55.6 1.0 copy-start.2
  63.0 101.1 %copy-start.9 = (bf16[1,2048,512]{2,1,0:T(8,128)(2,1)S(1)}, bf16[1,2048,512]{2,1,0:T(8,128)(2,1)}, u32[]{:S(2)}) copy-start(bf16[1,2048,512]{2,1,0:T(8,128)(2,1)} %param.25) | copy-start | bytes 6291460
  162.2 2.0 copy-start.1
  177.9 4.9 %copy-start.5 = (f32[256,2]{0,1:T(2,128)S(1)}, f32[256,2]{0,1:T(2,128)}, u32[]{:S(2)}) copy-start(f32[256,2]{0,1:T(2,128)} %param.24) | copy-start | bytes 6148
  177.9 4.9 %copy-start.8 = (f32[256]{0:T(256)S(1)}, f32[256]{0:T(256)}, u32[]{:S(2)}) copy-start(f32[256]{0:T(256)} %param.23) | copy-start | bytes 3076
  177.9 97.1 %all-to-all-start.2 = ((bf16[1,8,128,2048]{3,2,0,1:T(8,128)(2,1)}), bf16[1,8,128,2048]{3,2,0,1:T(8,128)(2,1)}, u32[]{:S(2)}, u32[]{:S(2)}) async-start(bf16[1,8,128,2048]{3,2,0,1:T(8,128)(2,1)} %convert_bitcast_fusion), calls=%async_computation.2 | async-start | bytes 8388608 | tf_op jit(solution)/shard_map/all_to_all | solution.py:87
  288.4 9.0 %copy-start.3 = (bf16[256,2048]{1,0:T(8,128)(2,1)S(1)}, bf16[256,2048]{1,0:T(8,128)(2,1)}, u32[]{:S(2)}) copy-start(bf16[256,2048]{1,0:T(8,128)(2,1)} %copy-done.2) | copy-start | bytes 3145732
Sparse Core Ops, SparseCore 0:
  8.9 42.7 all-gather.2
where the time goes:
time: 306 us; the launch traced here: 305 us
  waiting for transfers between devices  110 us (36%)
  blocking collectives  104 us (34%)
  local copies, waits for them, and re-layouts  28.5 us (9%)
  other arithmetic  18.2 us (6%)
  matrix products  17.6 us (6%)
  between operations  13.6 us (4%)
  starting transfers between devices  13.2 us (4%)
    all_to_all x1, blocking collectives, body(): lax.all_to_all(outgoing, 'sp', split_axis=1, concat_axis=1, tiled=True)  99.2 us
    all_to_all x1, waiting for transfers between devices, body(): lax.all_to_all(result, 'sp', split_axis=1, concat_axis=1, tiled=True)  92 us
    all_to_all x1, waiting for transfers between devices, body(): lax.all_to_all(mixed_out, 'tp', split_axis=0, concat_axis=1, tiled=True)  12.3 us
    dot_general x1, matrix products, body(): jnp.einsum('esrf,efd->esrd', hidden, expert_down, preferred_element_type=...  9.96 us
    reduce_sum x1, other arithmetic, body(): jnp.sum(slot_out.astype(jnp.float32) * weights[:, :, None], axis=1)  8.96 us
    gather x1, local copies, waits for them, and re-layouts, body(): returned.reshape(-1, width)[position].reshape(tok_rows, top_count, width)  7.96 us
  transfers between devices with their start and end apart: 4, of which 3 were waited for; matrix products, arithmetic and copies ran while one was open for 4% of the time, Pallas kernels for 0%

commit v1 on v0

v1 whole, which is shorter than its diff:
```python
import functools
import jax
import jax.numpy as jnp
from jax import lax
from jax.experimental import pallas as pl
from jax.experimental.pallas import tpu as pltpu
from jax.sharding import PartitionSpec as P

EPSILON = 1e-06


def from_behind(shard, axis, by):
    devices = lax.axis_size(axis)
    pairs = [(i, i + by) for i in range(devices) if 0 <= i + by < devices]
    return lax.ppermute(shard, axis, pairs)


def rms_norm(values, gain):
    floats = values.astype(jnp.float32)
    factor = lax.rsqrt(jnp.mean(floats * floats, axis=-1, keepdims=True) + EPSILON)
    return floats * factor * gain.astype(jnp.float32)


GATHER_BYTES = 26 * 2**20


def ffn_kernel(x_ref, w_ref, gate_ref, up_ref, down_ref, out_ref, acc_ref):
    step = pl.program_id(0)
    x = x_ref[...]
    gate = jnp.dot(x, gate_ref[0], preferred_element_type=jnp.float32)
    up = jnp.dot(x, up_ref[0], preferred_element_type=jnp.float32)
    hidden = (w_ref[0] * (jax.nn.silu(gate) * up)).astype(jnp.bfloat16)
    part = jnp.dot(hidden, down_ref[0], preferred_element_type=jnp.float32)

    @pl.when(step == 0)
    def _():
        acc_ref[...] = part

    @pl.when(step > 0)
    def _():
        acc_ref[...] += part

    @pl.when(step == pl.num_programs(0) - 1)
    def _():
        out_ref[...] = acc_ref[...].astype(out_ref.dtype)


def weighted_experts(x, w, gate, up, down, out_dtype):
    rows, width = x.shape
    pieces, _, units = gate.shape
    experts = w.shape[0]
    return pl.pallas_call(
        ffn_kernel,
        grid=(pieces,),
        in_specs=[
            pl.BlockSpec((rows, width), lambda g: (0, 0)),
            pl.BlockSpec((1, rows, 1), lambda g: (PIECE_EXPERT(g, experts, pieces), 0, 0)),
            pl.BlockSpec((1, width, units), lambda g: (g, 0, 0)),
            pl.BlockSpec((1, width, units), lambda g: (g, 0, 0)),
            pl.BlockSpec((1, units, width), lambda g: (g, 0, 0)),
        ],
        out_specs=pl.BlockSpec((rows, width), lambda g: (0, 0)),
        out_shape=jax.ShapeDtypeStruct((rows, width), out_dtype),
        scratch_shapes=[pltpu.VMEM((rows, width), jnp.float32)],
        compiler_params=pltpu.CompilerParams(dimension_semantics=("arbitrary",), vmem_limit_bytes=40 * 2**20),
        cost_estimate=pl.CostEstimate(
            flops=6 * rows * width * units * pieces,
            bytes_accessed=6 * pieces * width * units + 6 * rows * width,
            transcendentals=rows * units * pieces,
        ),
    )(x, w, gate, up, down)


def PIECE_EXPERT(g, experts, pieces):
    return g // (pieces // experts)


def half_slice(residual, routed_in, ids, group_prob, route_prob, gate, up, down):
    sp, tp = lax.axis_size("sp"), lax.axis_size("tp")
    half = sp // 2
    local = gate.shape[0]
    rows, width = routed_in.shape
    tp_me, sp_me = lax.axis_index("tp"), lax.axis_index("sp")
    units = gate.shape[2] // tp
    gate_cut = lax.dynamic_slice_in_dim(gate, tp_me * units, units, 2)
    up_cut = lax.dynamic_slice_in_dim(up, tp_me * units, units, 2)
    down_cut = lax.dynamic_slice_in_dim(down, tp_me * units, units, 1)
    groups = [[(h * half + s) * tp + t for s in range(half) for t in range(tp)] for h in range(2)]
    gather = functools.partial(
        lax.all_gather, axis_name=("sp", "tp"), axis_index_groups=groups, axis=0, tiled=True
    )
    gates, ups, downs = gather(gate_cut), gather(up_cut), gather(down_cut)
    experts_half = local * half
    assert local == 1
    pairs = [(i, (i + half) % sp) for i in range(sp)]
    weights = group_prob[:, None] * route_prob / jnp.sum(route_prob, axis=1, keepdims=True)
    dense = jnp.sum(
        jnp.where(
            ids[None, :, :] == jnp.arange(experts_half * 2, dtype=jnp.int32)[:, None, None],
            weights[None],
            0.0,
        ),
        axis=2,
    ).reshape(2, experts_half, rows)
    mine = lax.dynamic_index_in_dim(dense, sp_me // half, 0, keepdims=False)[:, :, None]
    other = lax.dynamic_index_in_dim(dense, 1 - sp_me // half, 0, keepdims=False)
    other = lax.ppermute(other, "sp", pairs)[:, :, None]
    across = lax.ppermute(routed_in, "sp", pairs)
    own = weighted_experts(routed_in, mine, gates, ups, downs, jnp.float32)
    theirs = weighted_experts(across, other, gates, ups, downs, jnp.bfloat16)
    back = lax.ppermute(theirs, "sp", pairs)
    return (residual.astype(jnp.float32) + own + back.astype(jnp.float32)).astype(jnp.bfloat16)


def exchange_slots(residual, routed_in, expert_ids, group_prob, route_prob, expert_gate, expert_up, expert_down):
    tok_rows, width = routed_in.shape
    top_count = expert_ids.shape[1]
    local_count = expert_gate.shape[0]
    group_count = lax.axis_size("sp")
    experts_all = local_count * group_count
    capacity = 2 * tok_rows * top_count // experts_all
    slots = tok_rows * top_count
    flat_e = expert_ids.reshape(-1)
    one_hot = (flat_e[:, None] == jnp.arange(experts_all, dtype=jnp.int32)[None, :]).astype(
        jnp.int32
    )
    slot_rank = jnp.sum((jnp.cumsum(one_hot, axis=0) - 1) * one_hot, axis=1)
    owner_dev = flat_e // local_count
    local_slot = flat_e % local_count
    position = (local_slot * group_count + owner_dev) * capacity + slot_rank
    source_slot = (
        jnp.full((experts_all * capacity,), slots, jnp.int32)
        .at[position]
        .set(jnp.arange(slots, dtype=jnp.int32))
    )
    rows_pad = jnp.concatenate([routed_in, jnp.zeros((1, width), jnp.bfloat16)], axis=0)
    outgoing = rows_pad[source_slot // top_count].reshape(local_count, group_count, capacity, width)
    arrived = lax.all_to_all(outgoing, "sp", split_axis=1, concat_axis=1, tiled=True)
    gate_act = jnp.einsum(
        "esrd,edf->esrf", arrived, expert_gate, preferred_element_type=jnp.float32
    )
    up_act = jnp.einsum("esrd,edf->esrf", arrived, expert_up, preferred_element_type=jnp.float32)
    hidden = (jax.nn.silu(gate_act) * up_act).astype(jnp.bfloat16)
    result = jnp.einsum(
        "esrf,efd->esrd", hidden, expert_down, preferred_element_type=jnp.float32
    ).astype(jnp.bfloat16)
    returned = lax.all_to_all(result, "sp", split_axis=1, concat_axis=1, tiled=True)
    slot_out = returned.reshape(-1, width)[position].reshape(tok_rows, top_count, width)
    weights = group_prob[:, None] * route_prob / jnp.sum(route_prob, axis=1, keepdims=True)
    expert_sum = jnp.sum(slot_out.astype(jnp.float32) * weights[:, :, None], axis=1)
    return (residual.astype(jnp.float32) + expert_sum).astype(jnp.bfloat16)


def body(
    residual_in,
    gate_outer,
    gate_inner,
    conv_input,
    conv_taps,
    norm_gain,
    out_weight,
    moe_gain,
    expert_ids,
    group_prob,
    route_prob,
    expert_gate,
    expert_up,
    expert_down,
):
    seq_rows, channels = conv_input.shape
    taps_count = conv_taps.shape[0]
    inner = gate_inner.astype(jnp.float32) * conv_input.astype(jnp.float32)
    earlier = from_behind(inner[seq_rows - (taps_count - 1) :], "sp", 1)
    padded = jnp.concatenate([earlier, inner], axis=0)
    tap_f = conv_taps.astype(jnp.float32)
    filtered = jnp.zeros((seq_rows, channels), jnp.float32)
    for offset in range(taps_count):
        filtered = filtered + tap_f[offset][None, :] * padded[offset : offset + seq_rows]
    mixed_out = (gate_outer.astype(jnp.float32) * filtered).astype(jnp.bfloat16)
    gathered = lax.all_to_all(mixed_out, "tp", split_axis=0, concat_axis=1, tiled=True)
    full_weight, full_gain = (
        lax.all_gather(out_weight, "tp", axis=0, tiled=True),
        lax.all_gather(norm_gain, "tp", axis=0, tiled=True),
    )
    normed = rms_norm(gathered, full_gain).astype(jnp.bfloat16)
    projected = jnp.dot(normed, full_weight, preferred_element_type=jnp.float32)
    residual = (residual_in.astype(jnp.float32) + projected).astype(jnp.bfloat16)
    routed_in = rms_norm(residual, moe_gain).astype(jnp.bfloat16)
    sp = lax.axis_size("sp")
    expert_bytes = 3 * expert_gate.size * expert_gate.dtype.itemsize
    fits = expert_gate.shape[0] == 1 and sp % 2 == 0 and expert_bytes * sp // 2 <= GATHER_BYTES
    experts = half_slice if fits else exchange_slots
    return experts(
        residual, routed_in, expert_ids, group_prob, route_prob, expert_gate, expert_up, expert_down
    )


def solution(mesh):
    in_specs = (
        P(("sp", "tp"), None),
        P("sp", "tp"),
        P("sp", "tp"),
        P("sp", "tp"),
        P(None, "tp"),
        P("tp"),
        P("tp", None),
        P(),
        P(("sp", "tp"), None),
        P(("sp", "tp")),
        P(("sp", "tp"), None),
        P("sp", None, None),
        P("sp", None, None),
        P("sp", None, None),
    )
    out_specs = P(("sp", "tp"), None)
    return jax.shard_map(body, mesh=mesh, in_specs=in_specs, out_specs=out_specs, check_vma=False)
```

time: 306 us -> 313 us (1.023)
  blocking collectives: 104 us -> 15.7 us
  waiting for transfers between devices: 110 us -> 193 us
  Pallas kernels: 0 us -> 44.7 us
  matrix products: 17.6 us -> 3.89 us
  other arithmetic: 18.2 us -> 7.04 us
  local copies, waits for them, and re-layouts: 28.5 us -> 20.1 us
    all_gather x0 -> x3, waiting for transfers between devices: none -> 120 us  [half_slice(): gates, ups, downs = (gather(gate_cut), gather(up_cut), gather(down_cut))]
    all_to_all x1 -> x0, blocking collectives: 99.2 us -> none  [body(): lax.all_to_all(outgoing, 'sp', split_axis=1, concat_axis=1, tiled=True)]
    all_to_all x1 -> x0, waiting for transfers between devices: 92 us -> none  [body(): lax.all_to_all(result, 'sp', split_axis=1, concat_axis=1, tiled=True)]
    ppermute x0 -> x3, waiting for transfers between devices: none -> 65.3 us  [the longest x1 45.8 us: half_slice(): other = lax.ppermute(other, 'sp', pairs)[:, :, None]]
    pallas_call x0 -> x2, Pallas kernels: none -> 44.7 us  [weighted_experts(): pl.pallas_call(ffn_kernel, grid=(pieces,), in_specs=[pl.BlockSpec((rows,...]
    gather x2 -> x0, local copies, waits for them, and re-layouts: 14 us -> none  [the longest x1 7.96 us: body(): returned.reshape(-1, width)[position].reshape(tok_rows, top_count, width)]
    dot_general x2 -> x0, matrix products: 13.7 us -> none  [the longest x1 9.96 us: body(): jnp.einsum('esrf,efd->esrd', hidden, expert_down, preferred_element_type=...]
    all_to_all x1, waiting for transfers between devices: 12.3 us -> 0.01 us  [body(): lax.all_to_all(mixed_out, 'tp', split_axis=0, concat_axis=1, tiled=True)]
  transfers between devices with their start and end apart: 4 -> 9, of which waited for: 3 -> 7; matrix products, arithmetic and copies ran while one was open for 4% -> 6% of each run, Pallas kernels for 0% -> 7%
where the time goes in v1:
time: 313 us; the launch traced here: 312 us
  waiting for transfers between devices  193 us (62%)
  Pallas kernels  44.7 us (14%)
  local copies, waits for them, and re-layouts  20.1 us (6%)
  blocking collectives  15.7 us (5%)
  starting transfers between devices  14.1 us (5%)
  between operations  13.4 us (4%)
  other arithmetic  7.04 us (2%)
  matrix products  3.89 us (1%)
    all_gather x3, waiting for transfers between devices, half_slice(): gates, ups, downs = (gather(gate_cut), gather(up_cut), gather(down_cut))  120 us
    ppermute x1, waiting for transfers between devices, half_slice(): other = lax.ppermute(other, 'sp', pairs)[:, :, None]  45.8 us
    pallas_call x2, Pallas kernels, weighted_experts(): pl.pallas_call(ffn_kernel, grid=(pieces,), in_specs=[pl.BlockSpec((rows,...  44.7 us
    ppermute x1, waiting for transfers between devices, half_slice(): back = lax.ppermute(theirs, 'sp', pairs)  19.4 us
    all_gather x1, blocking collectives, body(): lax.all_gather(norm_gain, 'tp', axis=0, tiled=True)  15.7 us
    unnamed x33, local copies, waits for them, and re-layouts  10.6 us
    all_gather x1, waiting for transfers between devices, body(): lax.all_gather(out_weight, 'tp', axis=0, tiled=True)  6.53 us
  transfers between devices with their start and end apart: 9, of which 7 were waited for; matrix products, arithmetic and copies ran while one was open for 6% of the time, Pallas kernels for 7%

profile of v1, /device:TPU:0, one launch (start us, length us, event | category | flops | bytes accessed | tf_op | source)
XLA Modules:
  0.0 312.2 jit_solution(13913408433224876611)
XLA Ops:
  6.5 0.7 all-gather.6.cloned.1.call-update
  7.3 0.8 copy-done
  8.1 0.9 constant_dynamic-slice_fusion.1
  9.1 2.0 constant_dynamic-slice_fusion
  11.1 1.9 constant_dynamic-slice_fusion.2
  13.2 5.0 %collective-permute-start = (f32[2,256]{1,0:T(2,128)S(1)}, f32[2,256]{1,0:T(2,128)S(1)}, u32[]{:S(2)}, u32[]{:S(2)}) collective-permute-start(f32[2,256]{1,0:T(2,128)S(1)} %slice.25), channel_id=1, source_target_pairs={{0,4},{4,8},{8,12},{12,16},{16,20},{20,24},{24,28},{1,5},{5,9},{9,... | collective-permute-start | bytes 6152 | tf_op jit(solution)/shard_map/ppermute | solution.py:15
  18.2 1.3 collective-permute-done
  19.5 1.2 fusion.11
  20.7 3.5 %all-to-all-start = ((bf16[4,256,256]{2,1,0:T(8,128)(2,1)}), bf16[4,256,256]{2,1,0:T(8,128)(2,1)S(1)}, u32[]{:S(2)}, u32[]{:S(2)}) async-start(bf16[4,256,256]{2,1,0:T(8,128)(2,1)} %bitcast.3), calls=%async_computation | async-start | bytes 1048576 | tf_op jit(solution)/shard_map/all_to_all | solution.py:180
  24.2 15.7 %all-gather = bf16[4,1,256]{2,1,0:T(2,128)(2,1)S(1)} all-gather(bf16[1,1,256]{2,1,0:T(2,128)(2,1)S(1)} %reshape.33), channel_id=1, replica_groups=mesh['sp'=8,'tp'=4] {'tp'}, dimensions={0}, use_global_device_ids=true | all-gather | bytes 2560 | tf_op jit(solution)/shard_map/all_gather | solution.py:183
  39.9 1.1 convert_bitcast_fusion
  41.0 2.6 copy.31
  43.8 1.4 fusion.15
  45.2 6.5 %all-gather.6.cloned.1.call-done = bf16[1024,2048]{1,0:T(8,128)(2,1)} async-done(((bf16[256,2048]{1,0:T(8,128)(2,1)}), bf16[1024,2048]{1,0:T(8,128)(2,1)}) %all-gather.6.cloned.1.call-update) | async-done | bytes 4194320 | tf_op jit(solution)/shard_map/all_gather | solution.py:182
  51.7 3.9 %fusion.1 = (f32[256]{0:T(256)S(1)}, bf16[256,2048]{1,0:T(8,128)(2,1)S(1)}) fusion(bf16[256,1024]{0,1:T(8,128)(2,1)S(1)} %fusion.15, bf16[1024,2048]{1,0:T(8,128)(2,1)} %all-gather.6.cloned.1.call-done, bf16[256,2048]{1,0:T(8,128)(2,1)} %param.14), kind=kOutput, calls=%fused_computation.5 | convolution fusion | flops 1076887296 | bytes 6816768 | tf_op jit(solution)/shard_map/dot_general | solution.py:186
  55.7 0.9 copy-done.5
  56.9 2.5 collective-permute-start.1
  60.1 45.8 %collective-permute-done.2 = f32[4,256]{1,0:T(4,128)S(1)} collective-permute-done((f32[4,256]{1,0:T(4,128)S(1)}, f32[4,256]{1,0:T(4,128)S(1)}, u32[]{:S(2)}, u32[]{:S(2)}) %collective-permute-start.2) | collective-permute-done | bytes 4128 | tf_op jit(solution)/shard_map/ppermute | solution.py:107
  105.9 1.1 copy.33.w_ref
  107.0 17.4 %all-gather.10.cloned.1.call-done.up_ref = bf16[16,2048,128]{2,1,0:T(8,128)(2,1)} async-done(((bf16[1,2048,128]{2,1,0:T(8,128)(2,1)}), bf16[16,2048,128]{2,1,0:T(8,128)(2,1)}) %all-gather.10.cloned.1.call-update) | async-done | bytes 8388624 | tf_op jit(solution)/shard_map/all_gather | solution.py:92
  124.4 51.1 %all-gather.12.cloned.1.call-done.down_ref = bf16[16,128,2048]{2,1,0:T(8,128)(2,1)} async-done(((bf16[1,128,2048]{2,1,0:T(8,128)(2,1)}), bf16[16,128,2048]{2,1,0:T(8,128)(2,1)}) %all-gather.12.cloned.1.call-update) | async-done | bytes 8388624 | tf_op jit(solution)/shard_map/all_gather | solution.py:92
  175.6 51.0 %all-gather.8.cloned.1.call-done.gate_ref = bf16[16,2048,128]{2,1,0:T(8,128)(2,1)} async-done(((bf16[1,2048,128]{2,1,0:T(8,128)(2,1)}), bf16[16,2048,128]{2,1,0:T(8,128)(2,1)}) %all-gather.8.cloned.1.call-update) | async-done | bytes 8388624 | tf_op jit(solution)/shard_map/all_gather | solution.py:92
  226.5 3.4 %copy-done.1 = bf16[16,2048,128]{2,1,0:T(8,128)(2,1)S(1)} copy-done((bf16[16,2048,128]{2,1,0:T(8,128)(2,1)S(1)}, bf16[16,2048,128]{2,1,0:T(8,128)(2,1)}, u32[]{:S(2)}) %copy-start.1) | copy-done | bytes 8388632
  229.9 1.0 copy-done.4
  231.0 23.0 %shard_map.137 = bf16[256,2048]{1,0:T(8,128)(2,1)} custom-call(bf16[256,2048]{1,0:T(8,128)(2,1)} %collective-permute-done.1.x_ref, f32[4,256,1]{2,1,0:T(8,128)S(1)} %copy-done.4, bf16[16,2048,128]{2,1,0:T(8,128)(2,1)S(1)} %copy-done.1, bf16[16,2048,128]{2,1,0:T(8,128)(2,1)} %all-gather.10.cloned.1.call-done.up_ref, ...), custom_call_target="tpu_custom_call" | custom-call | flops 6442450944 | bytes 28311552 | tf_op jit(solution)/shard_map/pallas_call | solution.py:52
  254.0 2.4 collective-permute-start.3
  256.4 1.0 copy.32.w_ref
  257.4 3.4 %copy-done.2 = bf16[16,2048,128]{2,1,0:T(8,128)(2,1)S(1)} copy-done((bf16[16,2048,128]{2,1,0:T(8,128)(2,1)S(1)}, bf16[16,2048,128]{2,1,0:T(8,128)(2,1)}, u32[]{:S(2)}) %copy-start.2) | copy-done | bytes 8388632
  260.8 1.0 copy-done.3
  261.8 21.7 %shard_map.136 = f32[256,2048]{1,0:T(8,128)S(1)} custom-call(bf16[256,2048]{1,0:T(8,128)(2,1)S(1)} %fusion.3.x_ref, f32[4,256,1]{2,1,0:T(8,128)S(1)} %copy-done.3, bf16[16,2048,128]{2,1,0:T(8,128)(2,1)S(1)} %copy-done.2, bf16[16,2048,128]{2,1,0:T(8,128)(2,1)} %all-gather.10.cloned.1.call-done.up_ref, ...), custom_call_target="tpu_custom_call" | custom-call | flops 6442450944 | bytes 28311552 | tf_op jit(solution)/shard_map/pallas_call | solution.py:52
  283.5 19.4 %collective-permute-done.3 = bf16[256,2048]{1,0:T(8,128)(2,1)} collective-permute-done((bf16[256,2048]{1,0:T(8,128)(2,1)}, bf16[256,2048]{1,0:T(8,128)(2,1)}, u32[]{:S(2)}, u32[]{:S(2)}) %collective-permute-start.3) | collective-permute-done | bytes 1048608 | tf_op jit(solution)/shard_map/ppermute | solution.py:111
  303.0 2.7 fusion.5
  (51 shorter events, 1.5 us)
Async XLA Ops:
  6.5 1.6 copy-start
  6.5 45.2 %all-gather.6.cloned.1.call-start = ((), (), s32[]{:S(2)}) async-start(), calls=%async_computation.1 | async-start | bytes 5242880 | tf_op jit(solution)/shard_map/all_gather | solution.py:182
  7.3 117.2 %all-gather.10.cloned.1.call-start = ((), (), s32[]{:S(2)}) async-start(), calls=%async_computation.3 | async-start | bytes 8912896 | tf_op jit(solution)/shard_map/all_gather | solution.py:92
  9.0 4.0 %copy-start.7 = (bf16[1024,256]{1,0:T(8,128)(2,1)S(1)}, bf16[1024,256]{1,0:T(8,128)(2,1)}, u32[]{:S(2)}) copy-start(bf16[1024,256]{1,0:T(8,128)(2,1)} %param.17) | copy-start | bytes 1572868
  9.0 4.0 %copy-start.8 = (bf16[1024,256]{1,0:T(8,128)(2,1)S(1)}, bf16[1024,256]{1,0:T(8,128)(2,1)}, u32[]{:S(2)}) copy-start(bf16[1024,256]{1,0:T(8,128)(2,1)} %param.16) | copy-start | bytes 1572868
  9.0 166.5 %all-gather.12.cloned.1.call-start = ((), (), s32[]{:S(2)}) async-start(), calls=%async_computation.4 | async-start | bytes 8912896 | tf_op jit(solution)/shard_map/all_gather | solution.py:92
  11.0 7.2 %copy-start.11 = (bf16[3,256]{1,0:T(4,128)(2,1)S(1)}, bf16[3,256]{1,0:T(4,128)(2,1)}, u32[]{:S(2)}) copy-start(bf16[3,256]{1,0:T(4,128)(2,1)} %param.18) | copy-start | bytes 4612
  11.1 215.5 %all-gather.8.cloned.1.call-start = ((), (), s32[]{:S(2)}) async-start(), calls=%async_computation.2 | async-start | bytes 8912896 | tf_op jit(solution)/shard_map/all_gather | solution.py:92
  13.0 6.5 %copy-start.9 = (bf16[1024,256]{1,0:T(8,128)(2,1)S(1)}, bf16[1024,256]{1,0:T(8,128)(2,1)}, u32[]{:S(2)}) copy-start(bf16[1024,256]{1,0:T(8,128)(2,1)} %param.15) | copy-start | bytes 1572868
  13.2 11.0 %copy-start.15 = (bf16[256]{0:T(256)(128)(2,1)S(1)}, bf16[256]{0:T(256)(128)(2,1)}, u32[]{:S(2)}) copy-start(bf16[256]{0:T(256)(128)(2,1)} %param.19) | copy-start | bytes 1540
  13.2 26.7 %copy-start.12 = (bf16[2048]{0:T(1024)(128)(2,1)S(1)}, bf16[2048]{0:T(1024)(128)(2,1)}, u32[]{:S(2)}) copy-start(bf16[2048]{0:T(1024)(128)(2,1)} %param.21) | copy-start | bytes 12292
  13.2 6.3 %collective-permute-start = (f32[2,256]{1,0:T(2,128)S(1)}, f32[2,256]{1,0:T(2,128)S(1)}, u32[]{:S(2)}, u32[]{:S(2)}) collective-permute-start(f32[2,256]{1,0:T(2,128)S(1)} %slice.25), channel_id=1, source_target_pairs={{0,4},{4,8},{8,12},{12,16},{16,20},{20,24},{24,28},{1,5},{5,9},{9,... | collective-permute-start | bytes 6152 | tf_op jit(solution)/shard_map/ppermute | solution.py:15
  20.7 19.2 %all-to-all-start = ((bf16[4,256,256]{2,1,0:T(8,128)(2,1)}), bf16[4,256,256]{2,1,0:T(8,128)(2,1)S(1)}, u32[]{:S(2)}, u32[]{:S(2)}) async-start(bf16[4,256,256]{2,1,0:T(8,128)(2,1)} %bitcast.3), calls=%async_computation | async-start | bytes 1048576 | tf_op jit(solution)/shard_map/all_to_all | solution.py:180
  55.6 1.0 copy-start.5
  55.7 3.8 %copy-start.10 = (f32[256,2]{0,1:T(2,128)S(1)}, f32[256,2]{0,1:T(2,128)}, u32[]{:S(2)}) copy-start(f32[256,2]{0,1:T(2,128)} %param.24) | copy-start | bytes 6148
  55.7 3.8 %copy-start.14 = (f32[256]{0:T(256)S(1)}, f32[256]{0:T(256)}, u32[]{:S(2)}) copy-start(f32[256]{0:T(256)} %param.23) | copy-start | bytes 3076
  55.7 3.8 %copy-start.13 = (s32[256,2]{0,1:T(2,128)S(1)}, s32[256,2]{0,1:T(2,128)}, u32[]{:S(2)}) copy-start(s32[256,2]{0,1:T(2,128)} %param.22) | copy-start | bytes 6148
  56.9 50.1 %collective-permute-start.1 = (bf16[256,2048]{1,0:T(8,128)(2,1)S(1)}, bf16[256,2048]{1,0:T(8,128)(2,1)}, u32[]{:S(2)}, u32[]{:S(2)}) collective-permute-start(bf16[256,2048]{1,0:T(8,128)(2,1)S(1)} %fusion.3.x_ref), channel_id=1, source_target_pairs={{0,16},{4,20},{8,24},{12,28},{16,0},{20,4},{24,8},{28,12},{1,17},{... | collective-permute-start | bytes 3145736 | tf_op jit(solution)/shard_map/ppermute | solution.py:108
  59.5 46.4 %collective-permute-start.2 = (f32[4,256]{1,0:T(4,128)S(1)}, f32[4,256]{1,0:T(4,128)S(1)}, u32[]{:S(2)}, u32[]{:S(2)}) collective-permute-start(f32[4,256]{1,0:T(4,128)S(1)} %get-tuple-element.5), channel_id=1, source_target_pairs={{0,16},{4,20},{8,24},{12,28},{16,0},{20,4},{24,8},{28,12},{1,17},{... | collective-permute-start | bytes 12296 | tf_op jit(solution)/shard_map/ppermute | solution.py:107
  226.5 3.4 %copy-start.1 = (bf16[16,2048,128]{2,1,0:T(8,128)(2,1)S(1)}, bf16[16,2048,128]{2,1,0:T(8,128)(2,1)}, u32[]{:S(2)}) copy-start(bf16[16,2048,128]{2,1,0:T(8,128)(2,1)} %all-gather.8.cloned.1.call-done.gate_ref) | copy-start | bytes 25165828
  229.9 1.0 copy-start.4
  254.0 49.0 %collective-permute-start.3 = (bf16[256,2048]{1,0:T(8,128)(2,1)}, bf16[256,2048]{1,0:T(8,128)(2,1)}, u32[]{:S(2)}, u32[]{:S(2)}) collective-permute-start(bf16[256,2048]{1,0:T(8,128)(2,1)} %shard_map.137), channel_id=1, source_target_pairs={{0,16},{4,20},{8,24},{12,28},{16,0},{20,4},{24,8},{28,12},{1,17},{... | collective-permute-start | bytes 3145736 | tf_op jit(solution)/shard_map/ppermute | solution.py:111
  257.4 3.4 %copy-start.2 = (bf16[16,2048,128]{2,1,0:T(8,128)(2,1)S(1)}, bf16[16,2048,128]{2,1,0:T(8,128)(2,1)}, u32[]{:S(2)}) copy-start(bf16[16,2048,128]{2,1,0:T(8,128)(2,1)} %all-gather.8.cloned.1.call-done.gate_ref) | copy-start | bytes 25165828
  260.8 1.0 copy-start.3
  261.8 41.1 %copy-start.6 = (bf16[256,2048]{1,0:T(8,128)(2,1)S(1)}, bf16[256,2048]{1,0:T(8,128)(2,1)}, u32[]{:S(2)}) copy-start(bf16[256,2048]{1,0:T(8,128)(2,1)} %copy-done.5) | copy-start | bytes 3145732
Sparse Core Ops, SparseCore 0:
  8.9 42.8 all-gather.5
  53.3 71.0 all-gather.9
  126.0 49.4 all-gather.11
  177.0 49.4 all-gather.7

commit v2 on v0

--- a/solution.py
+++ b/solution.py
@@ -1,6 +1,9 @@
+import functools
 import jax
 import jax.numpy as jnp
 from jax import lax
+from jax.experimental import pallas as pl
+from jax.experimental.pallas import tpu as pltpu
 from jax.sharding import PartitionSpec as P
 
 EPSILON = 1e-06
@@ -18,7 +21,237 @@
     return floats * factor * gain.astype(jnp.float32)
 
 
-def body(
+GATHER_BYTES = 26 * 2**20
+GAIN_ROWS = 16
+HALO_ROWS = 8
+
+
+def conv_kernel(outer_ref, inner_ref, input_ref, inner_back, input_back, halo_ref, taps_ref, gain_ref, out_ref):
+    rows = outer_ref.shape[0]
+    inner = inner_ref[...].astype(jnp.float32) * input_ref[...].astype(jnp.float32)
+    behind = inner_back[...].astype(jnp.float32) * input_back[...].astype(jnp.float32)
+    behind = behind[behind.shape[0] - HALO_ROWS :]
+    behind = jnp.where(pl.program_id(0) == 0, halo_ref[...], behind)
+    padded = jnp.concatenate([behind, inner], axis=0)
+    taps = taps_ref[...].astype(jnp.float32)
+    count = taps.shape[0]
+    filtered = jnp.zeros_like(inner)
+    for offset in range(count):
+        first = HALO_ROWS - (count - 1) + offset
+        filtered = filtered + taps[offset][None, :] * padded[first : first + rows]
+    mixed = (outer_ref[...].astype(jnp.float32) * filtered).astype(jnp.bfloat16)
+    out_ref[0, :rows] = mixed
+    out_ref[0, rows:] = jnp.broadcast_to(gain_ref[...], (GAIN_ROWS, mixed.shape[1]))
+
+
+def conv_blocks(outer, inner, values, halo, taps, gain, pieces):
+    rows, channels = outer.shape
+    block = rows // pieces
+    back = 2 * HALO_ROWS
+    main = pl.BlockSpec((block, channels), lambda b: (b, 0))
+    before = pl.BlockSpec((back, channels), lambda b: (jnp.maximum(b * (block // back) - 1, 0), 0))
+    whole = lambda a: pl.BlockSpec(a.shape, lambda b: (0, 0))
+    return pl.pallas_call(
+        conv_kernel,
+        grid=(pieces,),
+        in_specs=[main, main, main, before, before, whole(halo), whole(taps), whole(gain)],
+        out_specs=pl.BlockSpec((1, block + GAIN_ROWS, channels), lambda b: (b, 0, 0)),
+        out_shape=jax.ShapeDtypeStruct((pieces, block + GAIN_ROWS, channels), jnp.bfloat16),
+        cost_estimate=pl.CostEstimate(
+            flops=8 * rows * channels, bytes_accessed=8 * rows * channels, transcendentals=0
+        ),
+        compiler_params=pltpu.CompilerParams(vmem_limit_bytes=16 * 2**20),
+    )(outer, inner, values, inner, values, halo, taps, gain)
+
+
+def project_kernel(order, mixed_ref, *refs):
+    count = mixed_ref.shape[0]
+    weight_refs, (residual_ref, gain_ref, residual_out, routed_out) = refs[:count], refs[count:]
+    rows = residual_ref.shape[0]
+    channels = count * mixed_ref.shape[2]
+    me = lax.axis_index("tp")
+    total = jnp.zeros((rows, 1), jnp.float32)
+    for step in range(count):
+        block = mixed_ref[step, :rows].astype(jnp.float32)
+        total = total + jnp.sum(block * block, axis=1, keepdims=True)
+    factor = lax.rsqrt(total / channels + EPSILON)
+    out = residual_ref[...].astype(jnp.float32)
+    for step, weight_ref in zip(order, weight_refs):
+        block = mixed_ref[me ^ step]
+        gain = block[rows : rows + 1].astype(jnp.float32)
+        normed = (block[:rows].astype(jnp.float32) * factor * gain).astype(jnp.bfloat16)
+        out = out + jnp.dot(normed, weight_ref[...], preferred_element_type=jnp.float32)
+    residual = out.astype(jnp.bfloat16)
+    residual_out[...] = residual
+    floats = residual.astype(jnp.float32)
+    mean = jnp.mean(floats * floats, axis=1, keepdims=True)
+    routed = floats * lax.rsqrt(mean + EPSILON) * gain_ref[...].astype(jnp.float32)
+    routed_out[...] = routed.astype(jnp.bfloat16)
+
+
+def project(mixed, weights, order, residual_in, gain):
+    rows, width = residual_in.shape
+    vmem = pl.BlockSpec(memory_space=pltpu.VMEM)
+    shape = jax.ShapeDtypeStruct((rows, width), jnp.bfloat16)
+    return pl.pallas_call(
+        functools.partial(project_kernel, order),
+        in_specs=[vmem] * (len(weights) + 3),
+        out_specs=[vmem, vmem],
+        out_shape=[shape, shape],
+        cost_estimate=pl.CostEstimate(
+            flops=2 * rows * width * mixed.shape[0] * mixed.shape[2],
+            bytes_accessed=2 * width * mixed.shape[0] * mixed.shape[2] + 8 * rows * width,
+            transcendentals=0,
+        ),
+        compiler_params=pltpu.CompilerParams(vmem_limit_bytes=32 * 2**20),
+    )(mixed, *weights, residual_in, gain)
+
+
+def ffn_kernel(x_ref, y_ref, wx_ref, wy_ref, both_ref, down_ref, x_out, y_out, x_acc, y_acc):
+    step = pl.program_id(0)
+    cuts, units, width = down_ref.shape
+    down = down_ref[...].reshape(cuts * units, width)
+
+    def part(rows_ref, w_ref):
+        rows = rows_ref[...]
+        hidden = []
+        for cut in range(cuts):
+            act = jnp.dot(rows, both_ref[cut], preferred_element_type=jnp.float32)
+            gated = jax.nn.silu(act[:, :units]) * act[:, units:]
+            hidden.append((w_ref[0] * gated).astype(jnp.bfloat16))
+        hidden = jnp.concatenate(hidden, axis=1)
+        return jnp.dot(hidden, down, preferred_element_type=jnp.float32)
+
+    for rows_ref, w_ref, out_ref, acc_ref in (
+        (x_ref, wx_ref, x_out, x_acc),
+        (y_ref, wy_ref, y_out, y_acc),
+    ):
+        value = part(rows_ref, w_ref)
+
+        @pl.when(step == 0)
+        def _():
+            acc_ref[...] = value
+
+        @pl.when((step > 0) & (step < pl.num_programs(0) - 1))
+        def _():
+            acc_ref[...] += value
+
+        @pl.when(step == pl.num_programs(0) - 1)
+        def _():
+            out_ref[...] = (acc_ref[...] + value).astype(out_ref.dtype)
+
+
+def weighted_experts(x, y, wx, wy, both, down, x_dtype):
+    rows, width = x.shape
+    pieces, units, _ = down.shape
+    experts = wx.shape[0]
+    cuts = pieces // experts
+    full = pl.BlockSpec((rows, width), lambda e: (0, 0))
+    scale = pl.BlockSpec((1, rows, 1), lambda e: (e, 0, 0))
+    return pl.pallas_call(
+        ffn_kernel,
+        grid=(experts,),
+        in_specs=[
+            full,
+            full,
+            scale,
+            scale,
+            pl.BlockSpec((cuts, width, 2 * units), lambda e: (e, 0, 0)),
+            pl.BlockSpec((cuts, units, width), lambda e: (e, 0, 0)),
+        ],
+        out_specs=[full, full],
+        out_shape=[
+            jax.ShapeDtypeStruct((rows, width), x_dtype),
+            jax.ShapeDtypeStruct((rows, width), jnp.bfloat16),
+        ],
+        scratch_shapes=[pltpu.VMEM((rows, width), jnp.float32)] * 2,
+        compiler_params=pltpu.CompilerParams(
+            dimension_semantics=("arbitrary",), vmem_limit_bytes=40 * 2**20
+        ),
+        cost_estimate=pl.CostEstimate(
+            flops=12 * rows * width * units * pieces,
+            bytes_accessed=6 * pieces * width * units + 12 * rows * width,
+            transcendentals=2 * rows * units * pieces,
+        ),
+    )(x, y, wx, wy, both, down)
+
+
+def half_slice(
+    residual_in,
+    gate_outer,
+    gate_inner,
+    conv_input,
+    conv_taps,
+    norm_gain,
+    out_weight,
+    moe_gain,
+    expert_ids,
+    group_prob,
+    route_prob,
+    expert_gate,
+    expert_up,
+    expert_down,
+):
+    sp, tp = lax.axis_size("sp"), lax.axis_size("tp")
+    half, lanes = sp // 2, tp // 2
+    sp_me, tp_me = lax.axis_index("sp"), lax.axis_index("tp")
+    rows, width = residual_in.shape
+    core = [(i, i ^ 1) for i in range(tp)]
+    cross = [(i, (i + half) % sp) for i in range(sp)]
+
+    weights, order = [out_weight], [0]
+    for line in range(1, lanes):
+        pairs = [(i, i ^ (2 * line)) for i in range(tp)]
+        weights.append(lax.ppermute(out_weight, "tp", pairs))
+        order.append(2 * line)
+    weights += [lax.ppermute(block, "tp", core) for block in weights]
+    order += [step ^ 1 for step in order]
+
+    units = expert_gate.shape[2] // tp
+    first = ((tp_me % 2) * lanes + tp_me // 2) * units
+    gate_cut = lax.dynamic_slice_in_dim(expert_gate, first, units, 2)
+    up_cut = lax.dynamic_slice_in_dim(expert_up, first, units, 2)
+    down_cut = lax.dynamic_slice_in_dim(expert_down, first, units, 1)
+    groups = [
+        [(h * half + s) * tp + 2 * line + c for s in range(half) for line in range(lanes)]
+        for h in range(2)
+        for c in range(2)
+    ]
+    gather = functools.partial(
+        lax.all_gather, axis_name=("sp", "tp"), axis_index_groups=groups, axis=0, tiled=True
+    )
+    both = gather(jnp.concatenate([gate_cut, up_cut], axis=2))
+    down = gather(down_cut)
+
+    scale = group_prob[:, None] * route_prob / jnp.sum(route_prob, axis=1, keepdims=True)
+    experts = jnp.arange(sp, dtype=jnp.int32)[:, None, None]
+    dense = jnp.sum(jnp.where(expert_ids[None] == experts, scale[None], 0.0), axis=2)
+    pair = jnp.stack([dense, lax.ppermute(dense, "tp", core)]).reshape(2, 2, half, rows)
+    pick = lambda h: lax.dynamic_index_in_dim(pair, h, 1, keepdims=False)
+    near = pick(sp_me // half)[..., None]
+    far = lax.ppermute(pick(1 - sp_me // half), "sp", cross)[..., None]
+
+    taps = conv_taps.shape[0]
+    tail = gate_inner[-HALO_ROWS:].astype(jnp.float32) * conv_input[-HALO_ROWS:].astype(jnp.float32)
+    halo = from_behind(tail, "sp", 1)
+    mixed = conv_blocks(gate_outer, gate_inner, conv_input, halo, conv_taps, norm_gain[None], tp)
+    mixed = lax.all_to_all(mixed, "tp", split_axis=0, concat_axis=0, tiled=True)
+    residual, routed = project(mixed, weights, order, residual_in, moe_gain[None])
+
+    across = lax.ppermute(routed, "sp", cross)
+    beside = lax.ppermute(routed, "tp", core)
+    own, partner = weighted_experts(routed, beside, near[0], near[1], both, down, jnp.float32)
+    across_beside = lax.ppermute(across, "tp", core)
+    theirs, others = weighted_experts(
+        across, across_beside, far[0], far[1], both, down, jnp.float32
+    )
+    theirs = (theirs + lax.ppermute(others, "tp", core).astype(jnp.float32)).astype(jnp.bfloat16)
+    back = lax.ppermute(theirs, "sp", cross)
+    own = own + lax.ppermute(partner, "tp", core).astype(jnp.float32)
+    return (residual.astype(jnp.float32) + own + back.astype(jnp.float32)).astype(jnp.bfloat16)
+
+
+def exchange_slots(
     residual_in,
     gate_outer,
     gate_inner,
@@ -109,4 +342,14 @@
         P("sp", None, None),
     )
     out_specs = P(("sp", "tp"), None)
+    def body(*args):
+        gate, outer = args[11], args[1]
+        sp, tp = mesh.shape["sp"], mesh.shape["tp"]
+        gathered = 3 * gate.size * gate.dtype.itemsize * sp // 4
+        pairs = gate.shape[0] == 1 and sp % 2 == 0 and tp & (tp - 1) == 0 and tp > 1
+        sized = gate.shape[2] % (128 * tp) == 0 and outer.shape[0] % (16 * tp) == 0
+        if pairs and sized and gathered <= GATHER_BYTES:
+            return half_slice(*args)
+        return exchange_slots(*args)
+
     return jax.shard_map(body, mesh=mesh, in_specs=in_specs, out_specs=out_specs, check_vma=False)

time: 306 us -> 384 us (1.25)
  waiting for transfers between devices: 110 us -> 295 us
  blocking collectives: 104 us -> 0 us
  Pallas kernels: 0 us -> 30.3 us
  matrix products: 17.6 us -> 0 us
  other arithmetic: 18.2 us -> 4.35 us
  local copies, waits for them, and re-layouts: 28.5 us -> 17.2 us
  starting transfers between devices: 13.2 us -> 22.6 us
    ppermute x0 -> x11, waiting for transfers between devices: none -> 162 us  [the longest x1 65.7 us: half_slice(): weights.append(lax.ppermute(out_weight, 'tp', pairs))]
    all_gather x1 -> x2, waiting for transfers between devices: 5.02 us -> 109 us  [the longest x1 109 us: half_slice(): both = gather(jnp.concatenate([gate_cut, up_cut], axis=2))]
    all_to_all x1 -> x0, blocking collectives: 99.2 us -> none  [body(): lax.all_to_all(outgoing, 'sp', split_axis=1, concat_axis=1, tiled=True)]
    all_to_all x2 -> x1, waiting for transfers between devices: 104 us -> 23.2 us  [half_slice(): mixed = lax.all_to_all(mixed, 'tp', split_axis=0, concat_axis=0, tiled=True)]
    pallas_call x0 -> x4, Pallas kernels: none -> 30.3 us  [the longest x2 25 us: weighted_experts(): pl.pallas_call(ffn_kernel, grid=(experts,), in_specs=[full, full, scale,...]
    dot_general x3 -> x0, matrix products: 17.6 us -> none  [the longest x1 9.96 us: body(): jnp.einsum('esrf,efd->esrd', hidden, expert_down, preferred_element_type=...]
    ppermute x0 -> x11, starting transfers between devices: none -> 14.1 us  [the longest x1 5.45 us: half_slice(): across = lax.ppermute(routed, 'sp', cross)]
    gather x2 -> x0, local copies, waits for them, and re-layouts: 14 us -> none  [the longest x1 7.96 us: body(): returned.reshape(-1, width)[position].reshape(tok_rows, top_count, width)]
  transfers between devices with their start and end apart: 4 -> 15, of which waited for: 3 -> 8; matrix products, arithmetic and copies ran while one was open for 4% -> 1% of each run, Pallas kernels for 0% -> 8%
where the time goes in v2:
time: 384 us
  waiting for transfers between devices  295 us (77%)
  Pallas kernels  30.3 us (8%)
  starting transfers between devices  22.6 us (6%)
  local copies, waits for them, and re-layouts  17.2 us (4%)
  between operations  13.7 us (4%)
  other arithmetic  4.35 us (1%)
    all_gather x1, waiting for transfers between devices, half_slice(): both = gather(jnp.concatenate([gate_cut, up_cut], axis=2))  109 us
    ppermute x1, waiting for transfers between devices, half_slice(): weights.append(lax.ppermute(out_weight, 'tp', pairs))  65.7 us
    ppermute x1, waiting for transfers between devices, half_slice(): back = lax.ppermute(theirs, 'sp', cross)  46.1 us
    ppermute x1, waiting for transfers between devices, half_slice(): across = lax.ppermute(routed, 'sp', cross)  45.1 us
    pallas_call x2, Pallas kernels, weighted_experts(): pl.pallas_call(ffn_kernel, grid=(experts,), in_specs=[full, full, scale,...  25 us
    all_to_all x1, waiting for transfers between devices, half_slice(): mixed = lax.all_to_all(mixed, 'tp', split_axis=0, concat_axis=0, tiled=True)  23.2 us
    unnamed x41, local copies, waits for them, and re-layouts  14.1 us
  transfers between devices with their start and end apart: 15, of which 8 were waited for; matrix products, arithmetic and copies ran while one was open for 1% of the time, Pallas kernels for 8%

profile of v2, /device:TPU:0, one launch (start us, length us, event | category | flops | bytes accessed | tf_op | source)
XLA Modules:
  0.0 383.7 jit_solution(17059780059411613397)
XLA Ops:
  6.5 1.6 copy-done
  9.0 1.3 constant_dynamic-slice_fusion.1
  10.4 1.1 pad_maximum_fusion
  11.5 3.1 collective-permute-start.1
  14.6 65.7 %collective-permute-done.1.refs_1_ = bf16[256,2048]{1,0:T(8,128)(2,1)} collective-permute-done((bf16[256,2048]{1,0:T(8,128)(2,1)}, bf16[256,2048]{1,0:T(8,128)(2,1)}, u32[]{:S(2)}, u32[]{:S(2)}) %collective-permute-start.1) | collective-permute-done | bytes 1048608 | tf_op jit(solution)/shard_map/ppermute | solution.py:205
  80.3 4.7 %collective-permute-start = (f32[8,256]{1,0:T(8,128)S(1)}, f32[8,256]{1,0:T(8,128)S(1)}, u32[]{:S(2)}, u32[]{:S(2)}) collective-permute-start(f32[8,256]{1,0:T(8,128)S(1)} %convert_multiply_fusion), channel_id=1, source_target_pairs={{0,4},{4,8},{8,12},{12,16},{16,20},{20,24},{24,28},{1,5},{5,9},{9,... | collective-permute-start | bytes 24584 | tf_op jit(solution)/shard_map/ppermute | solution.py:15
  85.1 1.3 collective-permute-done.halo_ref
  86.4 1.0 copy-done.9
  87.5 1.8 shard_map.136
  89.2 3.7 all-to-all-start
  93.0 23.2 %all-to-all-done.mixed_ref = bf16[4,272,256]{2,1,0:T(8,128)(2,1)S(1)} async-done(((bf16[4,272,256]{2,1,0:T(8,128)(2,1)}), bf16[4,272,256]{2,1,0:T(8,128)(2,1)S(1)}, u32[]{:S(2)}, u32[]{:S(2)}) %all-to-all-start) | async-done | bytes 557088 | tf_op jit(solution)/shard_map/all_to_all | solution.py:238
  116.2 1.2 copy-done.5
  117.4 1.2 copy-done.6
  118.7 3.6 shard_map.137
  122.2 1.0 copy-done.7
  123.2 1.0 copy-done.13
  124.2 5.5 %collective-permute-start.7 = (bf16[256,2048]{1,0:T(8,128)(2,1)S(1)}, bf16[256,2048]{1,0:T(8,128)(2,1)}, u32[]{:S(2)}, u32[]{:S(2)}) collective-permute-start(bf16[256,2048]{1,0:T(8,128)(2,1)S(1)} %get-tuple-element.12.x_ref), channel_id=1, source_target_pairs={{0,16},{4,20},{8,24},{12,28},{16,0},{20,4},{24,8},{28,12},{1,17},{... | collective-permute-start | bytes 3145736 | tf_op jit(solution)/shard_map/ppermute | solution.py:241
  129.6 45.1 %collective-permute-done.7.x_ref = bf16[256,2048]{1,0:T(8,128)(2,1)} collective-permute-done((bf16[256,2048]{1,0:T(8,128)(2,1)S(1)}, bf16[256,2048]{1,0:T(8,128)(2,1)}, u32[]{:S(2)}, u32[]{:S(2)}) %collective-permute-start.7) | collective-permute-done | bytes 1048608 | tf_op jit(solution)/shard_map/ppermute | solution.py:241
  175.4 2.3 collective-permute-done.5
  177.8 1.9 collective-permute-start.9
  179.7 2.8 collective-permute-done.9
  183.1 108.9 %all-gather.3.cloned.1.call-done.both_ref = bf16[8,2048,256]{2,1,0:T(8,128)(2,1)} async-done(((bf16[1,2048,256]{2,1,0:T(8,128)(2,1)}), bf16[8,2048,256]{2,1,0:T(8,128)(2,1)}) %all-gather.3.cloned.1.call-update) | async-done | bytes 8388624 | tf_op jit(solution)/shard_map/all_gather | solution.py:223
  291.9 2.2 copy-done.11
  294.1 13.1 %shard_map.139 = (f32[256,2048]{1,0:T(8,128)S(1)}, bf16[256,2048]{1,0:T(8,128)(2,1)}) custom-call(bf16[256,2048]{1,0:T(8,128)(2,1)} %collective-permute-done.7.x_ref, bf16[256,2048]{1,0:T(8,128)(2,1)} %collective-permute-done.8.y_ref, f32[4,256,1]{2,1,0:T(8,128)S(1)} %copy.37.wx_ref, f32[4,256,1]{2,1,0:T(8,128)S(1)} %copy.38.wy_ref, ...), custom_call_target="tpu_custom_call" | custom-call | flops 6442450944 | bytes 18874368 | tf_op jit(solution)/shard_map/pallas_call | solution.py:151
  307.3 1.3 copy-done.3
  309.1 2.3 copy-done.12
  311.4 1.2 copy-done.14
  312.6 11.8 %shard_map.138 = (f32[256,2048]{1,0:T(8,128)S(1)}, bf16[256,2048]{1,0:T(8,128)(2,1)S(1)}) custom-call(bf16[256,2048]{1,0:T(8,128)(2,1)S(1)} %copy-done.14, bf16[256,2048]{1,0:T(8,128)(2,1)} %collective-permute-done.4.y_ref, f32[4,256,1]{2,1,0:T(8,128)S(1)} %copy.35.wx_ref, f32[4,256,1]{2,1,0:T(8,128)S(1)} %copy.36.wy_ref, ...), custom_call_target="tpu_custom_call" | custom-call | flops 6442450944 | bytes 18874368 | tf_op jit(solution)/shard_map/pallas_call | solution.py:151
  325.0 1.6 add_convert_fusion.1
  326.6 2.5 collective-permute-start.11
  329.1 46.1 %collective-permute-done.11 = bf16[256,2048]{1,0:T(8,128)(2,1)S(1)} collective-permute-done((bf16[256,2048]{1,0:T(8,128)(2,1)S(1)}, bf16[256,2048]{1,0:T(8,128)(2,1)S(1)}, u32[]{:S(2)}, u32[]{:S(2)}) %collective-permute-start.11) | collective-permute-done | bytes 1048608 | tf_op jit(solution)/shard_map/ppermute | solution.py:249
  375.2 1.6 add_convert_fusion
  (66 shorter events, 3.2 us)
Async XLA Ops:
  6.5 1.6 copy-start
  6.5 176.5 %all-gather.5.cloned.1.call-start = ((), (), s32[]{:S(2)}) async-start(), calls=%async_computation.2 | async-start | bytes 4718592 | tf_op jit(solution)/shard_map/all_gather | solution.py:224
  9.0 283.0 %all-gather.3.cloned.1.call-start = ((), (), s32[]{:S(2)}) async-start(), calls=%async_computation.1 | async-start | bytes 9437184 | tf_op jit(solution)/shard_map/all_gather | solution.py:223
  10.3 70.0 %copy-start.1 = (bf16[1024,256]{1,0:T(8,128)(2,1)S(1)}, bf16[1024,256]{1,0:T(8,128)(2,1)}, u32[]{:S(2)}) copy-start(bf16[1024,256]{1,0:T(8,128)(2,1)} %inner_back.1) | copy-start | bytes 1572868
  10.3 69.9 %copy-start.2 = (bf16[1024,256]{1,0:T(8,128)(2,1)S(1)}, bf16[1024,256]{1,0:T(8,128)(2,1)}, u32[]{:S(2)}) copy-start(bf16[1024,256]{1,0:T(8,128)(2,1)} %input_back.1) | copy-start | bytes 1572868
  10.4 74.7 %copy-start.19 = (bf16[256]{0:T(256)(128)(2,1)S(1)}, bf16[256]{0:T(256)(128)(2,1)}, u32[]{:S(2)}) copy-start(bf16[256]{0:T(256)(128)(2,1)} %param.19) | copy-start | bytes 1540
  10.4 76.0 %copy-start.10 = (bf16[3,256]{1,0:T(4,128)(2,1)S(1)}, bf16[3,256]{1,0:T(4,128)(2,1)}, u32[]{:S(2)}) copy-start(bf16[3,256]{1,0:T(4,128)(2,1)} %taps_ref.1) | copy-start | bytes 4612
  11.5 68.8 %collective-permute-start.1 = (bf16[256,2048]{1,0:T(8,128)(2,1)}, bf16[256,2048]{1,0:T(8,128)(2,1)}, u32[]{:S(2)}, u32[]{:S(2)}) collective-permute-start(bf16[256,2048]{1,0:T(8,128)(2,1)} %refs_0_.1), channel_id=1, source_target_pairs={{0,2},{1,3},{2,0},{3,1},{4,6},{5,7},{6,4},{7,5},{8,10},{9,11},{10,... | collective-permute-start | bytes 3145736 | tf_op jit(solution)/shard_map/ppermute | solution.py:205
  14.6 101.6 %collective-permute-start.2 = (bf16[256,2048]{1,0:T(8,128)(2,1)}, bf16[256,2048]{1,0:T(8,128)(2,1)}, u32[]{:S(2)}, u32[]{:S(2)}) collective-permute-start(bf16[256,2048]{1,0:T(8,128)(2,1)} %refs_0_.1), channel_id=1, source_target_pairs={{0,1},{1,0},{2,3},{3,2},{4,5},{5,4},{6,7},{7,6},{8,9},{9,8},{10,11... | collective-permute-start | bytes 3145736 | tf_op jit(solution)/shard_map/ppermute | solution.py:207
  80.3 35.9 %collective-permute-start.3 = (bf16[256,2048]{1,0:T(8,128)(2,1)}, bf16[256,2048]{1,0:T(8,128)(2,1)}, u32[]{:S(2)}, u32[]{:S(2)}) collective-permute-start(bf16[256,2048]{1,0:T(8,128)(2,1)} %collective-permute-done.1.refs_1_), channel_id=1, source_target_pairs={{0,1},{1,0},{2,3},{3,2},{4,5},{5,4},{6,7},{7,6},{8,9},{9,8},{10,11... | collective-permute-start | bytes 3145736 | tf_op jit(solution)/shard_map/ppermute | solution.py:207
  80.3 6.1 %collective-permute-start = (f32[8,256]{1,0:T(8,128)S(1)}, f32[8,256]{1,0:T(8,128)S(1)}, u32[]{:S(2)}, u32[]{:S(2)}) collective-permute-start(f32[8,256]{1,0:T(8,128)S(1)} %convert_multiply_fusion), channel_id=1, source_target_pairs={{0,4},{4,8},{8,12},{12,16},{16,20},{20,24},{24,28},{1,5},{5,9},{9,... | collective-permute-start | bytes 24584 | tf_op jit(solution)/shard_map/ppermute | solution.py:15
  87.5 5.5 %copy-start.16 = (bf16[2048]{0:T(1024)(128)(2,1)S(1)}, bf16[2048]{0:T(1024)(128)(2,1)}, u32[]{:S(2)}) copy-start(bf16[2048]{0:T(1024)(128)(2,1)} %param.21) | copy-start | bytes 12292
  89.2 26.9 %all-to-all-start = ((bf16[4,272,256]{2,1,0:T(8,128)(2,1)}), bf16[4,272,256]{2,1,0:T(8,128)(2,1)S(1)}, u32[]{:S(2)}, u32[]{:S(2)}) async-start(bf16[4,272,256]{2,1,0:T(8,128)(2,1)} %shard_map.136), calls=%async_computation | async-start | bytes 1114112 | tf_op jit(solution)/shard_map/all_to_all | solution.py:238
  93.0 81.8 %copy-start.15 = (f32[256,2]{0,1:T(2,128)S(1)}, f32[256,2]{0,1:T(2,128)}, u32[]{:S(2)}) copy-start(f32[256,2]{0,1:T(2,128)} %param.24) | copy-start | bytes 6148
  93.0 81.8 %copy-start.18 = (f32[256]{0:T(256)S(1)}, f32[256]{0:T(256)}, u32[]{:S(2)}) copy-start(f32[256]{0:T(256)} %param.23) | copy-start | bytes 3076
  93.0 81.8 %copy-start.17 = (s32[256,2]{0,1:T(2,128)S(1)}, s32[256,2]{0,1:T(2,128)}, u32[]{:S(2)}) copy-start(s32[256,2]{0,1:T(2,128)} %param.22) | copy-start | bytes 6148
  116.2 1.2 copy-start.5
  117.4 1.2 copy-start.6
  124.2 50.5 %collective-permute-start.7 = (bf16[256,2048]{1,0:T(8,128)(2,1)S(1)}, bf16[256,2048]{1,0:T(8,128)(2,1)}, u32[]{:S(2)}, u32[]{:S(2)}) collective-permute-start(bf16[256,2048]{1,0:T(8,128)(2,1)S(1)} %get-tuple-element.12.x_ref), channel_id=1, source_target_pairs={{0,16},{4,20},{8,24},{12,28},{16,0},{20,4},{24,8},{28,12},{1,17},{... | collective-permute-start | bytes 3145736 | tf_op jit(solution)/shard_map/ppermute | solution.py:241
  174.7 8.3 %collective-permute-start.8 = (bf16[256,2048]{1,0:T(8,128)(2,1)}, bf16[256,2048]{1,0:T(8,128)(2,1)}, u32[]{:S(2)}, u32[]{:S(2)}) collective-permute-start(bf16[256,2048]{1,0:T(8,128)(2,1)} %collective-permute-done.7.x_ref), channel_id=1, source_target_pairs={{0,1},{1,0},{2,3},{3,2},{4,5},{5,4},{6,7},{7,6},{8,9},{9,8},{10,11... | collective-permute-start | bytes 3145736 | tf_op jit(solution)/shard_map/ppermute | solution.py:244
  174.8 2.9 collective-permute-start.5
  177.8 4.7 %collective-permute-start.9 = (f32[2,4,256]{2,1,0:T(4,128)S(1)}, f32[2,4,256]{2,1,0:T(4,128)S(1)}, u32[]{:S(2)}, u32[]{:S(2)}) collective-permute-start(f32[2,4,256]{2,1,0:T(4,128)S(1)} %dynamic-slice_bitcast_fusion), channel_id=1, source_target_pairs={{0,16},{4,20},{8,24},{12,28},{16,0},{20,4},{24,8},{28,12},{1,17},{... | collective-permute-start | bytes 24584 | tf_op jit(solution)/shard_map/ppermute | solution.py:232
  182.9 126.1 %collective-permute-start.4 = (bf16[256,2048]{1,0:T(8,128)(2,1)}, bf16[256,2048]{1,0:T(8,128)(2,1)}, u32[]{:S(2)}, u32[]{:S(2)}) collective-permute-start(bf16[256,2048]{1,0:T(8,128)(2,1)} %copy-done.13), channel_id=1, source_target_pairs={{0,1},{1,0},{2,3},{3,2},{4,5},{5,4},{6,7},{7,6},{8,9},{9,8},{10,11... | collective-permute-start | bytes 3145736 | tf_op jit(solution)/shard_map/ppermute | solution.py:242
  291.9 2.2 copy-start.11
  307.3 1.3 copy-start.3
  308.6 16.5 %collective-permute-start.10 = (bf16[256,2048]{1,0:T(8,128)(2,1)}, bf16[256,2048]{1,0:T(8,128)(2,1)}, u32[]{:S(2)}, u32[]{:S(2)}) collective-permute-start(bf16[256,2048]{1,0:T(8,128)(2,1)} %get-tuple-element.16), channel_id=1, source_target_pairs={{0,1},{1,0},{2,3},{3,2},{4,5},{5,4},{6,7},{7,6},{8,9},{9,8},{10,11... | collective-permute-start | bytes 3145736 | tf_op jit(solution)/shard_map/ppermute | solution.py:248
  309.0 16.0 %copy-start.4 = (f32[256,2048]{1,0:T(8,128)S(1)}, f32[256,2048]{1,0:T(8,128)}, u32[]{:S(2)}) copy-start(f32[256,2048]{1,0:T(8,128)} %copy-done.3) | copy-start | bytes 6291460
  309.1 2.3 copy-start.12
  311.4 1.2 copy-start.14
  324.5 4.7 %collective-permute-start.6 = (bf16[256,2048]{1,0:T(8,128)(2,1)S(1)}, bf16[256,2048]{1,0:T(8,128)(2,1)S(1)}, u32[]{:S(2)}, u32[]{:S(2)}) collective-permute-start(bf16[256,2048]{1,0:T(8,128)(2,1)S(1)} %get-tuple-element.14), channel_id=1, source_target_pairs={{0,1},{1,0},{2,3},{3,2},{4,5},{5,4},{6,7},{7,6},{8,9},{9,8},{10,11... | collective-permute-start | bytes 3145736 | tf_op jit(solution)/shard_map/ppermute | solution.py:250
  325.0 50.1 %copy-start.8 = (bf16[256,2048]{1,0:T(8,128)(2,1)S(1)}, bf16[256,2048]{1,0:T(8,128)(2,1)}, u32[]{:S(2)}) copy-start(bf16[256,2048]{1,0:T(8,128)(2,1)} %copy-done.7) | copy-start | bytes 3145732
  326.6 48.5 %collective-permute-start.11 = (bf16[256,2048]{1,0:T(8,128)(2,1)S(1)}, bf16[256,2048]{1,0:T(8,128)(2,1)S(1)}, u32[]{:S(2)}, u32[]{:S(2)}) collective-permute-start(bf16[256,2048]{1,0:T(8,128)(2,1)S(1)} %add_convert_fusion.1), channel_id=1, source_target_pairs={{0,16},{4,20},{8,24},{12,28},{16,0},{20,4},{24,8},{28,12},{1,17},{... | collective-permute-start | bytes 3145736 | tf_op jit(solution)/shard_map/ppermute | solution.py:249
  (3 other events, 3.0 us)
Sparse Core Ops, SparseCore 0:
  9.1 114.1 all-gather.4
  124.9 167.0 all-gather.2

commit v3 on v0

--- a/solution.py
+++ b/solution.py
@@ -1,8 +1,12 @@
+import functools
 import jax
 import jax.numpy as jnp
 from jax import lax
+from jax.experimental import pallas as pl
+from jax.experimental.pallas import tpu as pltpu
 from jax.sharding import PartitionSpec as P
 
+MESH = pl.DeviceIdType.MESH
 EPSILON = 1e-06
 
 
@@ -18,7 +22,300 @@
     return floats * factor * gain.astype(jnp.float32)
 
 
-def body(
+GATHER_BYTES = 26 * 2**20
+GAIN_ROWS = 16
+HALO_ROWS = 16
+
+
+def mixer_kernel(
+    outer_ref, inner_ref, input_ref, taps_ref, gain_ref, weight_ref, residual_ref, moe_ref, near_ref, far_ref,
+    both_ref, down_ref,
+    residual_out, routed_out, across_out, beside_out, across_beside_out,
+    near_beside_out, far_out, far_beside_out, both_out, down_out,
+    halo, sent, got, weights, send_sem, recv_sem,
+):
+    sp, tp = lax.axis_index("sp"), lax.axis_index("tp")
+    sp_size, tp_size = lax.axis_size("sp"), lax.axis_size("tp")
+    core_bit = 1 - 2 * (tp % 2)
+    line_bit = 2 - 4 * ((tp // 2) % 2)
+    lanes = [tp, tp + core_bit, tp + line_bit, tp + line_bit + core_bit]
+    core, line = (sp, lanes[1]), (sp, lanes[2])
+    x_peer = (sp + 1 - 2 * (sp % 2), tp)
+    z_peer = (sp + 2 - 4 * ((sp // 2) % 2), tp)
+    cross = ((sp + sp_size // 2) % sp_size, tp)
+    after, before = ((sp + 1) % sp_size, tp), ((sp + sp_size - 1) % sp_size, tp)
+    peers = [core, line, (sp, lanes[3]), x_peer, z_peer, cross, after, before]
+
+    barrier = pltpu.get_barrier_semaphore()
+    for peer in peers:
+        pl.semaphore_signal(barrier, inc=1, device_id=peer, device_id_type=MESH)
+    pl.semaphore_wait(barrier, len(peers))
+
+    started = []
+
+    def send(source, target, peer):
+        number = len(started)
+        copy = pltpu.make_async_remote_copy(
+            src_ref=source, dst_ref=target, send_sem=send_sem.at[number], recv_sem=recv_sem.at[number],
+            device_id=peer, device_id_type=MESH,
+        )
+        copy.start()
+        started.append(copy)
+        return copy
+
+    full = inner_ref.shape[0]
+    halos = [
+        send(inner_ref.at[pl.ds(full - HALO_ROWS, HALO_ROWS)], halo.at[0], after),
+        send(input_ref.at[pl.ds(full - HALO_ROWS, HALO_ROWS)], halo.at[1], after),
+    ]
+    weight_line = send(weight_ref, weights.at[1], line)
+    weight_core = send(weight_ref, weights.at[0], core)
+
+    def pieces(source_both, source_down, slot, piece, peer):
+        return [
+            send(source_both, both_out.at[slot, piece], peer),
+            send(source_down, down_out.at[slot, piece], peer),
+        ]
+
+    x_first = pieces(both_ref.at[0], down_ref.at[0], 0, 0, x_peer)
+    z_first = pieces(both_ref.at[1], down_ref.at[1], 1, 1, z_peer)
+    x_second = pieces(both_ref.at[1], down_ref.at[1], 0, 1, x_peer)
+    z_second = pieces(both_ref.at[0], down_ref.at[0], 1, 0, z_peer)
+    near_copy = send(near_ref, near_beside_out, core)
+    far_copy = send(far_ref, far_out, cross)
+
+    for copy in halos:
+        copy.wait_recv()
+    rows = residual_ref.shape[0]
+    taps = taps_ref[...].astype(jnp.float32)
+    count = taps.shape[0]
+    exchanged = []
+    for step in (2, 3, 1, 0):
+        block = lanes[step]
+        first = pl.multiple_of(block * rows, rows)
+        inner = inner_ref[pl.ds(first, rows)].astype(jnp.float32) * input_ref[pl.ds(first, rows)].astype(jnp.float32)
+        back = pl.multiple_of(jnp.maximum(block * rows - HALO_ROWS, 0), HALO_ROWS)
+        behind = inner_ref[pl.ds(back, HALO_ROWS)].astype(jnp.float32) * input_ref[pl.ds(back, HALO_ROWS)].astype(jnp.float32)
+        outside = halo[0].astype(jnp.float32) * halo[1].astype(jnp.float32)
+        outside = jnp.where(sp == 0, 0.0, outside)
+        behind = jnp.where(block == 0, outside, behind)
+        padded = jnp.concatenate([behind, inner], axis=0)
+        filtered = jnp.zeros_like(inner)
+        for offset in range(count):
+            start = HALO_ROWS - (count - 1) + offset
+            filtered = filtered + taps[offset][None, :] * padded[start : start + rows]
+        mixed = (outer_ref[pl.ds(first, rows)].astype(jnp.float32) * filtered).astype(jnp.bfloat16)
+        sent[step, :rows] = mixed
+        sent[step, rows:] = jnp.broadcast_to(gain_ref[...], (GAIN_ROWS, mixed.shape[1]))
+        if step > 0:
+            exchanged.append(send(sent.at[step], got.at[step - 1], (sp, block)))
+
+    for copy in exchanged:
+        copy.wait_recv()
+    blocks = [sent.at[0], got.at[0], got.at[1], got.at[2]]
+    total = jnp.zeros((rows, 1), jnp.float32)
+    for block in blocks:
+        values = block[:rows].astype(jnp.float32)
+        total = total + jnp.sum(values * values, axis=1, keepdims=True)
+    factor = lax.rsqrt(total / (tp_size * inner_ref.shape[1]) + EPSILON)
+
+    def normed(block):
+        gain = block[rows:][:1].astype(jnp.float32)
+        return (block[:rows].astype(jnp.float32) * factor * gain).astype(jnp.bfloat16)
+
+    weight_line.wait_recv()
+    weight_both = send(weights.at[1], weights.at[2], core)
+    far_copy.wait_recv()
+    far_beside = send(far_out, far_beside_out, core)
+    weight_core.wait_recv()
+    width = residual_ref.shape[1]
+    out = residual_ref[...].astype(jnp.float32)
+    out = out + jnp.dot(normed(blocks[0]), weight_ref[...], preferred_element_type=jnp.float32)
+    out = out + jnp.dot(normed(blocks[1]), weights[0], preferred_element_type=jnp.float32)
+    out = out + jnp.dot(normed(blocks[2]), weights[1], preferred_element_type=jnp.float32)
+    weight_both.wait_recv()
+    out = out + jnp.dot(normed(blocks[3]), weights[2], preferred_element_type=jnp.float32)
+    residual = out.astype(jnp.bfloat16)
+    residual_out[...] = residual
+    floats = residual.astype(jnp.float32)
+    mean = jnp.mean(floats * floats, axis=1, keepdims=True)
+    routed = floats * lax.rsqrt(mean + EPSILON) * moe_ref[...].astype(jnp.float32)
+    routed_out[...] = routed.astype(jnp.bfloat16)
+
+    across = send(routed_out, across_out, cross)
+    beside = send(routed_out, beside_out, core)
+    for copy in x_first:
+        copy.wait_recv()
+    diagonal = pieces(both_out.at[0, 0], down_out.at[0, 0], 2, 0, z_peer)
+    for copy in z_first:
+        copy.wait_recv()
+    diagonal += pieces(both_out.at[1, 1], down_out.at[1, 1], 2, 1, x_peer)
+    across.wait_recv()
+    across_beside = send(across_out, across_beside_out, core)
+    late = x_second + z_second + [near_copy, far_beside, beside, across_beside] + diagonal
+    for copy in late:
+        copy.wait_recv()
+    for copy in started:
+        copy.wait_send()
+
+
+COPIES = 26
+
+
+def mixer(outer, inner, values, taps, gain, weight, residual_in, moe_gain, near, far, both, down):
+    rows, width = residual_in.shape
+    channels = outer.shape[1]
+    tp = lax.axis_size("tp")
+    vmem = pl.BlockSpec(memory_space=pltpu.VMEM)
+    hbm = pl.BlockSpec(memory_space=pl.ANY)
+    tokens = jax.ShapeDtypeStruct((rows, width), jnp.bfloat16)
+    scale = jax.ShapeDtypeStruct(near.shape, near.dtype)
+    return pl.pallas_call(
+        mixer_kernel,
+        in_specs=[vmem] * 10 + [hbm] * 2,
+        out_specs=[vmem, vmem, hbm, hbm, hbm, vmem, vmem, vmem, hbm, hbm],
+        out_shape=[tokens] * 5
+        + [scale] * 3
+        + [jax.ShapeDtypeStruct((3,) + a.shape, a.dtype) for a in (both, down)],
+        scratch_shapes=[
+            pltpu.VMEM((2, HALO_ROWS, channels), jnp.bfloat16),
+            pltpu.VMEM((tp, rows + GAIN_ROWS, channels), jnp.bfloat16),
+            pltpu.VMEM((tp - 1, rows + GAIN_ROWS, channels), jnp.bfloat16),
+            pltpu.VMEM((tp - 1,) + weight.shape, jnp.bfloat16),
+            pltpu.SemaphoreType.DMA((COPIES,)),
+            pltpu.SemaphoreType.DMA((COPIES,)),
+        ],
+        compiler_params=pltpu.CompilerParams(
+            collective_id=0, has_side_effects=True, vmem_limit_bytes=48 * 2**20
+        ),
+    )(outer, inner, values, taps, gain, weight, residual_in, moe_gain, near, far, both, down)
+
+
+def ffn_kernel(x_ref, y_ref, wx_ref, wy_ref, own_both, own_down, both_ref, down_ref, x_out, y_out, x_acc, y_acc):
+    step = pl.program_id(0)
+    cuts, units, width = own_down.shape
+
+    def part(rows_ref, w_ref, both, down):
+        rows = rows_ref[...]
+        hidden = []
+        for cut in range(cuts):
+            act = jnp.dot(rows, both[cut], preferred_element_type=jnp.float32)
+            gated = jax.nn.silu(act[:, :units]) * act[:, units:]
+            hidden.append((w_ref[0] * gated).astype(jnp.bfloat16))
+        hidden = jnp.concatenate(hidden, axis=1)
+        return jnp.dot(hidden, down[...].reshape(cuts * units, width), preferred_element_type=jnp.float32)
+
+    tokens = ((x_ref, wx_ref, x_out, x_acc), (y_ref, wy_ref, y_out, y_acc))
+
+    @pl.when(step == 0)
+    def _():
+        for rows_ref, w_ref, _, acc_ref in tokens:
+            acc_ref[...] = part(rows_ref, w_ref, own_both, own_down)
+
+    @pl.when(step > 0)
+    def _():
+        for rows_ref, w_ref, _, acc_ref in tokens:
+            acc_ref[...] += part(rows_ref, w_ref, both_ref.at[0], down_ref.at[0])
+
+    @pl.when(step == pl.num_programs(0) - 1)
+    def _():
+        for _, _, out_ref, acc_ref in tokens:
+            out_ref[...] = acc_ref[...].astype(out_ref.dtype)
+
+
+def weighted_experts(x, y, wx, wy, own_both, own_down, both, down):
+    rows, width = x.shape
+    cuts, units, _ = own_down.shape
+    experts = wx.shape[0]
+    full = pl.BlockSpec((rows, width), lambda e: (0, 0))
+    scale = pl.BlockSpec((1, rows, 1), lambda e: (e, 0, 0))
+    whole = lambda a: pl.BlockSpec(a.shape, lambda e: (0, 0, 0))
+    other = lambda a: pl.BlockSpec((1,) + a.shape[1:], lambda e: (jnp.maximum(e - 1, 0), 0, 0, 0))
+    return pl.pallas_call(
+        ffn_kernel,
+        grid=(experts,),
+        in_specs=[full, full, scale, scale, whole(own_both), whole(own_down), other(both), other(down)],
+        out_specs=[full, full],
+        out_shape=[
+            jax.ShapeDtypeStruct((rows, width), jnp.float32),
+            jax.ShapeDtypeStruct((rows, width), jnp.bfloat16),
+        ],
+        scratch_shapes=[pltpu.VMEM((rows, width), jnp.float32)] * 2,
+        compiler_params=pltpu.CompilerParams(
+            dimension_semantics=("arbitrary",), vmem_limit_bytes=44 * 2**20
+        ),
+        cost_estimate=pl.CostEstimate(
+            flops=12 * rows * width * units * cuts * experts,
+            bytes_accessed=6 * cuts * experts * width * units + 12 * rows * width,
+            transcendentals=2 * rows * units * cuts * experts,
+        ),
+    )(x, y, wx, wy, own_both, own_down, both, down)
+
+
+def half_slice(
+    residual_in,
+    gate_outer,
+    gate_inner,
+    conv_input,
+    conv_taps,
+    norm_gain,
+    out_weight,
+    moe_gain,
+    expert_ids,
+    group_prob,
+    route_prob,
+    expert_gate,
+    expert_up,
+    expert_down,
+):
+    sp, tp = lax.axis_size("sp"), lax.axis_size("tp")
+    half, lanes = sp // 2, tp // 2
+    sp_me, tp_me = lax.axis_index("sp"), lax.axis_index("tp")
+    rows, width = residual_in.shape
+    core = [(i, i ^ 1) for i in range(tp)]
+    cross = [(i, (i + half) % sp) for i in range(sp)]
+
+    units = expert_gate.shape[2] // tp
+    first = (tp_me % 2) * lanes * units
+    cut = lambda a, start, axis: lax.dynamic_slice_in_dim(a, first + start, units, axis)
+    own_both, own_down = [], []
+    for piece in range(lanes):
+        start = piece * units
+        own_both += [cut(expert_gate, start, 2), cut(expert_up, start, 2)]
+        own_down.append(cut(expert_down, start, 1))
+    own_both = jnp.concatenate(
+        [jnp.concatenate(own_both[2 * p : 2 * p + 2], axis=2) for p in range(lanes)], axis=0
+    )
+    own_down = jnp.concatenate(own_down, axis=0)
+
+    scale = group_prob[:, None] * route_prob / jnp.sum(route_prob, axis=1, keepdims=True)
+    side = (sp_me % half) ^ jnp.arange(half, dtype=jnp.int32)
+    near_of = (sp_me // half) * half + side
+    far_of = (1 - sp_me // half) * half + side
+
+    def dense(experts):
+        return jnp.sum(jnp.where(expert_ids[None] == experts[:, None, None], scale[None], 0.0), axis=2)
+
+    near, far = dense(near_of), dense(far_of)
+    (
+        residual, routed, across, beside, across_beside, near_beside, far, far_beside, both, down
+    ) = mixer(
+        gate_outer, gate_inner, conv_input, conv_taps, norm_gain[None], out_weight, residual_in,
+        moe_gain[None], near, far, own_both, own_down,
+    )
+    column = lambda w: w[..., None]
+    experts = functools.partial(
+        weighted_experts, own_both=own_both, own_down=own_down, both=both, down=down
+    )
+    theirs, others = experts(across, across_beside, column(far), column(far_beside))
+    theirs = (theirs + lax.ppermute(others, "tp", core).astype(jnp.float32)).astype(jnp.bfloat16)
+    back = lax.ppermute(theirs, "sp", cross)
+    own, partner = experts(routed, beside, column(near), column(near_beside))
+    own = own + lax.ppermute(partner, "tp", core).astype(jnp.float32)
+    return (residual.astype(jnp.float32) + own + back.astype(jnp.float32)).astype(jnp.bfloat16)
+
+
+def exchange_slots(
     residual_in,
     gate_outer,
     gate_inner,
@@ -109,4 +406,14 @@
         P("sp", None, None),
     )
     out_specs = P(("sp", "tp"), None)
+    def body(*args):
+        gate, outer = args[11], args[1]
+        sp, tp = mesh.shape["sp"], mesh.shape["tp"]
+        gathered = 3 * gate.size * gate.dtype.itemsize * sp // 4
+        pairs = gate.shape[0] == 1 and sp == 8 and tp == 4
+        sized = gate.shape[2] % (128 * tp) == 0 and outer.shape[0] % (16 * tp) == 0
+        if pairs and sized and gathered <= GATHER_BYTES:
+            return half_slice(*args)
+        return exchange_slots(*args)
+
     return jax.shard_map(body, mesh=mesh, in_specs=in_specs, out_specs=out_specs, check_vma=False)

time: 306 us -> 237 us (0.77)
  Pallas kernels: 0 us -> 158 us
  blocking collectives: 104 us -> 0 us
  waiting for transfers between devices: 110 us -> 47.8 us
  matrix products: 17.6 us -> 0 us
  between operations: 13.6 us -> 0.11 us
  starting transfers between devices: 13.2 us -> 0.86 us
  other arithmetic: 18.2 us -> 7.3 us
  local copies, waits for them, and re-layouts: 28.5 us -> 23 us
    pallas_call x0 -> x3, Pallas kernels: none -> 158 us  [the longest x1 136 us: mixer(): pl.pallas_call(mixer_kernel, in_specs=[vmem] * 10 + [hbm] * 2, out_specs=...]
    all_to_all x2 -> x0, waiting for transfers between devices: 104 us -> none  [the longest x1 92 us: body(): lax.all_to_all(result, 'sp', split_axis=1, concat_axis=1, tiled=True)]
    all_to_all x1 -> x0, blocking collectives: 99.2 us -> none  [body(): lax.all_to_all(outgoing, 'sp', split_axis=1, concat_axis=1, tiled=True)]
    ppermute x1 -> x3, waiting for transfers between devices: 0.01 us -> 47.8 us  [the longest x1 47.4 us: half_slice(): back = lax.ppermute(theirs, 'sp', cross)]
    dot_general x3 -> x0, matrix products: 17.6 us -> none  [the longest x1 9.96 us: body(): jnp.einsum('esrf,efd->esrd', hidden, expert_down, preferred_element_type=...]
    gather x2 -> x0, local copies, waits for them, and re-layouts: 14 us -> none  [the longest x1 7.96 us: body(): returned.reshape(-1, width)[position].reshape(tok_rows, top_count, width)]
    unnamed x24 -> x46, local copies, waits for them, and re-layouts: 3.1 us -> 14.7 us
    reduce_sum x4 -> x2, other arithmetic: 9.25 us -> 0.78 us  [the longest x1 0.7 us: half_slice(): jnp.sum(route_prob, axis=1, keepdims=True)]
  transfers between devices with their start and end apart: 4 -> 3, of which waited for: 3 -> 2; matrix products, arithmetic and copies ran while one was open for 4% -> 2% of each run, Pallas kernels for 0% -> 4%
where the time goes in v3:
time: 237 us
  Pallas kernels  158 us (67%)
  waiting for transfers between devices  47.8 us (20%)
  local copies, waits for them, and re-layouts  23 us (10%)
  other arithmetic  7.3 us (3%)
    pallas_call x1, Pallas kernels, mixer(): pl.pallas_call(mixer_kernel, in_specs=[vmem] * 10 + [hbm] * 2, out_specs=...  136 us
    ppermute x1, waiting for transfers between devices, half_slice(): back = lax.ppermute(theirs, 'sp', cross)  47.4 us
    pallas_call x2, Pallas kernels, weighted_experts(): pl.pallas_call(ffn_kernel, grid=(experts,), in_specs=[full, full, scale,...  21.4 us
    unnamed x46, local copies, waits for them, and re-layouts  14.7 us
  transfers between devices with their start and end apart: 3, of which 2 were waited for; matrix products, arithmetic and copies ran while one was open for 2% of the time, Pallas kernels for 4%

profile of v3, /device:TPU:0, one launch (start us, length us, event | category | flops | bytes accessed | tf_op | source)
XLA Modules:
  0.0 236.8 jit_solution(9930838665472671753)
XLA Ops:
  0.0 0.8 broadcast_in_dim.42.gain_ref
  0.8 0.7 broadcast_in_dim.43.moe_ref
  1.5 0.7 reduce_sum.27
  2.2 0.7 multiply_divide_fusion
  2.9 1.3 constant_dynamic-slice_fusion.1
  4.2 1.5 constant_dynamic-slice_fusion.4
  5.7 1.1 pad_maximum_fusion.down_ref.own_down
  6.8 1.5 maximum_maximum_fusion.both_ref.own_both
  8.7 136.4 %shard_map.136 = (bf16[256,2048]{1,0:T(8,128)(2,1)S(1)}, bf16[256,2048]{1,0:T(8,128)(2,1)S(1)}, bf16[256,2048]{1,0:T(8,128)(2,1)S(1)}, bf16[256,2048]{1,0:T(8,12...) custom-call(bf16[1024,256]{1,0:T(8,128)(2,1)S(1)} %copy-done.10, ...), custom_call_target="tpu_custom_call" | custom-call | tf_op jit(solution)/shard_map/pallas_call | solution.py:173
  145.0 1.0 copy-done.4
  146.0 1.0 copy-done.14
  147.1 1.0 copy-done.16
  148.1 1.0 copy-done.18
  149.0 1.1 copy.25.wx_ref
  150.1 1.0 copy.26.wy_ref
  151.1 1.0 copy-done.8
  152.2 1.0 copy-done.9
  153.2 1.2 copy-done.19
  154.4 1.2 copy-done.20
  155.7 11.1 %shard_map.138 = (f32[256,2048]{1,0:T(8,128)S(1)}, bf16[256,2048]{1,0:T(8,128)(2,1)}) custom-call(bf16[256,2048]{1,0:T(8,128)(2,1)S(1)} %copy-done.19, bf16[256,2048]{1,0:T(8,128)(2,1)S(1)} %copy-done.20, f32[4,256,1]{2,1,0:T(8,128)S(1)} %copy-done.8, f32[4,256,1]{2,1,0:T(8,128)S(1)} %copy-done.9, bf16[2,2048,256]{2,1,0:T(8,128)(2,1)S(1)} %copy-done, ...), custom_call_target="tpu_custom_call" | custom-call | flops 6442450944 | bytes 18874368 | tf_op jit(solution)/shard_map/pallas_call | solution.py:234
  166.8 1.3 copy-done.2
  168.1 1.0 copy.23.wx_ref
  169.1 1.0 copy.24.wy_ref
  170.1 1.0 copy-done.6
  171.2 1.0 copy-done.7
  172.2 1.2 copy-done.15
  173.4 1.2 copy-done.17
  174.6 10.3 %shard_map.137 = (f32[256,2048]{1,0:T(8,128)S(1)}, bf16[256,2048]{1,0:T(8,128)(2,1)S(1)}) custom-call(bf16[256,2048]{1,0:T(8,128)(2,1)S(1)} %copy-done.15, bf16[256,2048]{1,0:T(8,128)(2,1)S(1)} %copy-done.17, f32[4,256,1]{2,1,0:T(8,128)S(1)} %copy-done.6, f32[4,256,1]{2,1,0:T(8,128)S(1)} %copy-done.7, bf16[2,2048,256]{2,1,0:T(8,128)(2,1)S(1)} %copy-done, ...), custom_call_target="tpu_custom_call" | custom-call | flops 6442450944 | bytes 18874368 | tf_op jit(solution)/shard_map/pallas_call | solution.py:234
  184.9 0.6 collective-permute-start
  185.5 1.6 add_convert_fusion.1
  187.8 47.4 %collective-permute-done.2 = bf16[256,2048]{1,0:T(8,128)(2,1)S(1)} collective-permute-done((bf16[256,2048]{1,0:T(8,128)(2,1)S(1)}, bf16[256,2048]{1,0:T(8,128)(2,1)S(1)}, u32[]{:S(2)}, u32[]{:S(2)}) %collective-permute-start.2) | collective-permute-done | bytes 1048608 | tf_op jit(solution)/shard_map/ppermute | solution.py:312
  235.2 1.6 add_convert_fusion
  (39 shorter events, 1.1 us)
Async XLA Ops:
  0.0 4.2 %copy-start.21 = (bf16[1,2048,512]{2,1,0:T(8,128)(2,1)S(1)}, bf16[1,2048,512]{2,1,0:T(8,128)(2,1)}, u32[]{:S(2)}) copy-start(bf16[1,2048,512]{2,1,0:T(8,128)(2,1)} %param.26) | copy-start | bytes 6291460
  5.6 1.1 copy-start.22
  6.8 1.6 copy-start.10
  6.8 1.6 copy-start.11
  6.8 1.9 copy-start.12
  6.8 1.8 copy-start.13
  8.7 142.5 %copy-start = (bf16[2,2048,256]{2,1,0:T(8,128)(2,1)S(1)}, bf16[2,2048,256]{2,1,0:T(8,128)(2,1)}, u32[]{:S(2)}) copy-start(bf16[2,2048,256]{2,1,0:T(8,128)(2,1)} %maximum_maximum_fusion.both_ref.own_both) | copy-start | bytes 6291460
  8.7 142.5 %copy-start.1 = (bf16[2,128,2048]{2,1,0:T(8,128)(2,1)S(1)}, bf16[2,128,2048]{2,1,0:T(8,128)(2,1)}, u32[]{:S(2)}) copy-start(bf16[2,128,2048]{2,1,0:T(8,128)(2,1)} %pad_maximum_fusion.down_ref.own_down) | copy-start | bytes 3145732
  145.0 1.0 copy-start.4
  146.0 1.0 copy-start.14
  147.1 1.0 copy-start.16
  148.1 1.0 copy-start.18
  151.1 1.0 copy-start.8
  152.2 1.0 copy-start.9
  153.2 1.2 copy-start.19
  154.4 1.2 copy-start.20
  166.8 1.3 copy-start.2
  168.1 17.4 %collective-permute-start.1 = (bf16[256,2048]{1,0:T(8,128)(2,1)}, bf16[256,2048]{1,0:T(8,128)(2,1)}, u32[]{:S(2)}, u32[]{:S(2)}) collective-permute-start(bf16[256,2048]{1,0:T(8,128)(2,1)} %get-tuple-element.32), channel_id=1, source_target_pairs={{0,1},{1,0},{2,3},{3,2},{4,5},{5,4},{6,7},{7,6},{8,9},{9,8},{10,11... | collective-permute-start | bytes 3145736 | tf_op jit(solution)/shard_map/ppermute | solution.py:311
  170.1 1.0 copy-start.6
  171.1 1.0 copy-start.7
  172.2 1.2 copy-start.15
  173.4 1.2 copy-start.17
  174.6 10.9 %copy-start.3 = (f32[256,2048]{1,0:T(8,128)S(1)}, f32[256,2048]{1,0:T(8,128)}, u32[]{:S(2)}) copy-start(f32[256,2048]{1,0:T(8,128)} %copy-done.2) | copy-start | bytes 6291460
  184.9 2.9 %collective-permute-start = (bf16[256,2048]{1,0:T(8,128)(2,1)S(1)}, bf16[256,2048]{1,0:T(8,128)(2,1)S(1)}, u32[]{:S(2)}, u32[]{:S(2)}) collective-permute-start(bf16[256,2048]{1,0:T(8,128)(2,1)S(1)} %get-tuple-element.26), channel_id=1, source_target_pairs={{0,1},{1,0},{2,3},{3,2},{4,5},{5,4},{6,7},{7,6},{8,9},{9,8},{10,11... | collective-permute-start | bytes 3145736 | tf_op jit(solution)/shard_map/ppermute | solution.py:314
  185.5 49.7 %copy-start.5 = (bf16[256,2048]{1,0:T(8,128)(2,1)S(1)}, bf16[256,2048]{1,0:T(8,128)(2,1)}, u32[]{:S(2)}) copy-start(bf16[256,2048]{1,0:T(8,128)(2,1)} %copy-done.4) | copy-start | bytes 3145732
  187.1 48.1 %collective-permute-start.2 = (bf16[256,2048]{1,0:T(8,128)(2,1)S(1)}, bf16[256,2048]{1,0:T(8,128)(2,1)S(1)}, u32[]{:S(2)}, u32[]{:S(2)}) collective-permute-start(bf16[256,2048]{1,0:T(8,128)(2,1)S(1)} %add_convert_fusion.1), channel_id=1, source_target_pairs={{0,16},{4,20},{8,24},{12,28},{16,0},{20,4},{24,8},{28,12},{1,17},{... | collective-permute-start | bytes 3145736 | tf_op jit(solution)/shard_map/ppermute | solution.py:312

commit v4 on v3

--- a/solution.py
+++ b/solution.py
@@ -5,6 +5,7 @@
 from jax.experimental import pallas as pl
 from jax.experimental.pallas import tpu as pltpu
 from jax.sharding import PartitionSpec as P
+
 
 MESH = pl.DeviceIdType.MESH
 EPSILON = 1e-06
@@ -77,10 +78,11 @@
             send(source_down, down_out.at[slot, piece], peer),
         ]
 
-    x_first = pieces(both_ref.at[0], down_ref.at[0], 0, 0, x_peer)
-    z_first = pieces(both_ref.at[1], down_ref.at[1], 1, 1, z_peer)
-    x_second = pieces(both_ref.at[1], down_ref.at[1], 0, 1, x_peer)
-    z_second = pieces(both_ref.at[0], down_ref.at[0], 1, 0, z_peer)
+    mine = (tp // 2) % 2
+    rest = 1 - mine
+    x_first = pieces(both_ref.at[mine], down_ref.at[mine], 0, mine, x_peer)
+    z_first = pieces(both_ref.at[mine], down_ref.at[mine], 1, mine, z_peer)
+    x_second = pieces(both_ref.at[rest], down_ref.at[rest], 0, rest, x_peer)
     near_copy = send(near_ref, near_beside_out, core)
     far_copy = send(far_ref, far_out, cross)
 
@@ -128,7 +130,6 @@
     far_copy.wait_recv()
     far_beside = send(far_out, far_beside_out, core)
     weight_core.wait_recv()
-    width = residual_ref.shape[1]
     out = residual_ref[...].astype(jnp.float32)
     out = out + jnp.dot(normed(blocks[0]), weight_ref[...], preferred_element_type=jnp.float32)
     out = out + jnp.dot(normed(blocks[1]), weights[0], preferred_element_type=jnp.float32)
@@ -142,18 +143,23 @@
     routed = floats * lax.rsqrt(mean + EPSILON) * moe_ref[...].astype(jnp.float32)
     routed_out[...] = routed.astype(jnp.bfloat16)
 
+    beside = send(routed_out, beside_out, core)
+    for copy in z_first:
+        copy.wait_recv()
+    z_second = pieces(both_out.at[1, mine], down_out.at[1, mine], 1, mine, line)
+    for copy in x_first:
+        copy.wait_recv()
+    diagonal = pieces(both_out.at[0, mine], down_out.at[0, mine], 2, mine, z_peer)
     across = send(routed_out, across_out, cross)
-    beside = send(routed_out, beside_out, core)
-    for copy in x_first:
-        copy.wait_recv()
-    diagonal = pieces(both_out.at[0, 0], down_out.at[0, 0], 2, 0, z_peer)
-    for copy in z_first:
-        copy.wait_recv()
-    diagonal += pieces(both_out.at[1, 1], down_out.at[1, 1], 2, 1, x_peer)
+    for copy in z_second:
+        copy.wait_recv()
+    last_down = send(down_out.at[1, rest], down_out.at[2, rest], x_peer)
+    for copy in diagonal:
+        copy.wait_recv()
+    last_both = send(both_out.at[2, mine], both_out.at[2, mine], line)
     across.wait_recv()
     across_beside = send(across_out, across_beside_out, core)
-    late = x_second + z_second + [near_copy, far_beside, beside, across_beside] + diagonal
-    for copy in late:
+    for copy in x_second + [near_copy, far_beside, beside, last_down, last_both, across_beside]:
         copy.wait_recv()
     for copy in started:
         copy.wait_send()
@@ -197,11 +203,12 @@
 
     def part(rows_ref, w_ref, both, down):
         rows = rows_ref[...]
+        scale = w_ref[pl.ds(step, 1), :].T
         hidden = []
         for cut in range(cuts):
             act = jnp.dot(rows, both[cut], preferred_element_type=jnp.float32)
             gated = jax.nn.silu(act[:, :units]) * act[:, units:]
-            hidden.append((w_ref[0] * gated).astype(jnp.bfloat16))
+            hidden.append((scale * gated).astype(jnp.bfloat16))
         hidden = jnp.concatenate(hidden, axis=1)
         return jnp.dot(hidden, down[...].reshape(cuts * units, width), preferred_element_type=jnp.float32)
 
@@ -228,7 +235,7 @@
     cuts, units, _ = own_down.shape
     experts = wx.shape[0]
     full = pl.BlockSpec((rows, width), lambda e: (0, 0))
-    scale = pl.BlockSpec((1, rows, 1), lambda e: (e, 0, 0))
+    scale = pl.BlockSpec(wx.shape, lambda e: (0, 0))
     whole = lambda a: pl.BlockSpec(a.shape, lambda e: (0, 0, 0))
     other = lambda a: pl.BlockSpec((1,) + a.shape[1:], lambda e: (jnp.maximum(e - 1, 0), 0, 0, 0))
     return pl.pallas_call(
@@ -242,7 +249,7 @@
         ],
         scratch_shapes=[pltpu.VMEM((rows, width), jnp.float32)] * 2,
         compiler_params=pltpu.CompilerParams(
-            dimension_semantics=("arbitrary",), vmem_limit_bytes=44 * 2**20
+            dimension_semantics=("arbitrary",), vmem_limit_bytes=60 * 2**20
         ),
         cost_estimate=pl.CostEstimate(
             flops=12 * rows * width * units * cuts * experts,
@@ -271,7 +278,6 @@
     sp, tp = lax.axis_size("sp"), lax.axis_size("tp")
     half, lanes = sp // 2, tp // 2
     sp_me, tp_me = lax.axis_index("sp"), lax.axis_index("tp")
-    rows, width = residual_in.shape
     core = [(i, i ^ 1) for i in range(tp)]
     cross = [(i, (i + half) % sp) for i in range(sp)]
 
@@ -303,14 +309,14 @@
         gate_outer, gate_inner, conv_input, conv_taps, norm_gain[None], out_weight, residual_in,
         moe_gain[None], near, far, own_both, own_down,
     )
-    column = lambda w: w[..., None]
     experts = functools.partial(
         weighted_experts, own_both=own_both, own_down=own_down, both=both, down=down
     )
-    theirs, others = experts(across, across_beside, column(far), column(far_beside))
+    theirs, others = experts(across, across_beside, far, far_beside)
     theirs = (theirs + lax.ppermute(others, "tp", core).astype(jnp.float32)).astype(jnp.bfloat16)
+    near, theirs = lax.optimization_barrier((near, theirs))
     back = lax.ppermute(theirs, "sp", cross)
-    own, partner = experts(routed, beside, column(near), column(near_beside))
+    own, partner = experts(routed, beside, near, near_beside)
     own = own + lax.ppermute(partner, "tp", core).astype(jnp.float32)
     return (residual.astype(jnp.float32) + own + back.astype(jnp.float32)).astype(jnp.bfloat16)
 
@@ -406,9 +412,10 @@
         P("sp", None, None),
     )
     out_specs = P(("sp", "tp"), None)
+    sp, tp = mesh.shape["sp"], mesh.shape["tp"]
+
     def body(*args):
         gate, outer = args[11], args[1]
-        sp, tp = mesh.shape["sp"], mesh.shape["tp"]
         gathered = 3 * gate.size * gate.dtype.itemsize * sp // 4
         pairs = gate.shape[0] == 1 and sp == 8 and tp == 4
         sized = gate.shape[2] % (128 * tp) == 0 and outer.shape[0] % (16 * tp) == 0

time: 237 us -> 222 us (0.937)
  local copies, waits for them, and re-layouts: 23 us -> 8.5 us
  Pallas kernels: 158 us -> 152 us
  waiting for transfers between devices: 47.8 us -> 51.7 us
    pallas_call x1, Pallas kernels: 136 us -> 125 us  [mixer(): pl.pallas_call(mixer_kernel, in_specs=[vmem] * 10 + [hbm] * 2, out_specs=...]
    unnamed x46 -> x28, local copies, waits for them, and re-layouts: 14.7 us -> 5.36 us
    pallas_call x2, Pallas kernels: 21.4 us -> 27 us  [weighted_experts(): pl.pallas_call(ffn_kernel, grid=(experts,), in_specs=[full, full, scale,...]
    broadcast_in_dim x4 -> x0, local copies, waits for them, and re-layouts: 4.13 us -> none  [half_slice(): column = lambda w: w[..., None]]
    ppermute x1, waiting for transfers between devices: 0.01 us -> 2.87 us  [half_slice(): lax.ppermute(others, 'tp', core).astype(jnp.float32)]
  transfers between devices with their start and end apart: 3 -> 3, of which waited for: 2 -> 3; matrix products, arithmetic and copies ran while one was open for 2% -> 0% of each run, Pallas kernels for 4% -> 0%
where the time goes in v4:
time: 222 us
  Pallas kernels  152 us (68%)
  waiting for transfers between devices  51.7 us (23%)
  other arithmetic  9.21 us (4%)
  local copies, waits for them, and re-layouts  8.5 us (4%)
    pallas_call x1, Pallas kernels, mixer(): pl.pallas_call(mixer_kernel, in_specs=[vmem] * 10 + [hbm] * 2, out_specs=...  125 us
    ppermute x1, waiting for transfers between devices, half_slice(): back = lax.ppermute(theirs, 'sp', cross)  46.1 us
    pallas_call x2, Pallas kernels, weighted_experts(): pl.pallas_call(ffn_kernel, grid=(experts,), in_specs=[full, full, scale,...  27 us
    unnamed x28, local copies, waits for them, and re-layouts  5.36 us
  transfers between devices with their start and end apart: 3, of which 3 were waited for; matrix products, arithmetic and copies ran while one was open for 0% of the time, Pallas kernels for 0%

profile of v4, /device:TPU:0, one launch (start us, length us, event | category | flops | bytes accessed | tf_op | source)
XLA Modules:
  0.0 221.9 jit_solution(3894459181011001989)
XLA Ops:
  0.0 0.7 broadcast_in_dim.30.gain_ref
  0.7 0.7 broadcast_in_dim.31.moe_ref
  1.4 0.7 reduce_sum.27
  2.1 0.7 multiply_divide_fusion
  2.8 1.4 constant_dynamic-slice_fusion.1
  4.2 1.1 pad_maximum_fusion.down_ref.own_down
  5.3 0.1 copy-done.12
  5.4 0.4 constant_dynamic-slice_fusion.4
  5.7 0.3 copy-done.13
  6.0 0.1 select_reduce_fusion
  6.1 0.0 copy-start.1
  6.1 0.0 copy-start.2
  6.2 0.0 copy-start.4
  6.2 1.5 maximum_maximum_fusion.both_ref.own_both
  7.7 0.2 copy-done.2
  8.0 125.2 %shard_map.136 = (bf16[256,2048]{1,0:T(8,128)(2,1)S(1)}, bf16[256,2048]{1,0:T(8,128)(2,1)S(1)}, bf16[256,2048]{1,0:T(8,128)(2,1)S(1)}, bf16[256,2048]{1,0:T(8,12...) custom-call(bf16[1024,256]{1,0:T(8,128)(2,1)S(1)} %copy-done, ...), custom_call_target="tpu_custom_call" | custom-call | tf_op jit(solution)/shard_map/pallas_call | solution.py:179
  133.2 1.0 copy-done.5
  134.2 1.0 copy-done.6
  135.2 1.0 copy-done.7
  136.1 0.6 copy-done.8
  136.7 0.6 copy-done.9
  137.3 0.6 copy-done.10
  137.9 13.6 %shard_map.137 = (f32[256,2048]{1,0:T(8,128)}, bf16[256,2048]{1,0:T(8,128)(2,1)}) custom-call(bf16[256,2048]{1,0:T(8,128)(2,1)} %copy-done.7, bf16[256,2048]{1,0:T(8,128)(2,1)} %get-tuple-element.25.y_ref, f32[4,256]{1,0:T(4,128)} %copy-done.9, f32[4,256]{1,0:T(4,128)} %copy-done.10, bf16[2,2048,256]{2,1,0:T(8,128)(2,1)} %maximum_maximum_fusion.both_ref.own_both, ...), custom_call_target="tpu_custom_call" | custom-call | flops 6442450944 | bytes 18874368 | tf_op jit(solution)/shard_map/pallas_call | solution.py:241
  151.5 0.0 collective-permute-start
  151.5 2.9 %collective-permute-done = bf16[256,2048]{1,0:T(8,128)(2,1)S(1)} collective-permute-done((bf16[256,2048]{1,0:T(8,128)(2,1)}, bf16[256,2048]{1,0:T(8,128)(2,1)S(1)}, u32[]{:S(2)}, u32[]{:S(2)}) %collective-permute-start) | collective-permute-done | bytes 1048608 | tf_op jit(solution)/shard_map/ppermute | solution.py:316
  154.3 1.9 add_convert_fusion.1
  156.2 13.5 %shard_map.138 = (f32[256,2048]{1,0:T(8,128)}, bf16[256,2048]{1,0:T(8,128)(2,1)}) custom-call(bf16[256,2048]{1,0:T(8,128)(2,1)} %copy-done.5, bf16[256,2048]{1,0:T(8,128)(2,1)} %copy-done.6, f32[4,256]{1,0:T(4,128)} %copy-done.3, f32[4,256]{1,0:T(4,128)} %copy-done.8, bf16[2,2048,256]{2,1,0:T(8,128)(2,1)} %maximum_maximum_fusion.both_ref.own_both, ...), custom_call_target="tpu_custom_call" | custom-call | flops 6442450944 | bytes 18874368 | tf_op jit(solution)/shard_map/pallas_call | solution.py:241
  169.7 0.1 collective-permute-start.1
  169.9 0.0 collective-permute-start.2
  169.9 2.7 %collective-permute-done.1 = bf16[256,2048]{1,0:T(8,128)(2,1)S(1)} collective-permute-done((bf16[256,2048]{1,0:T(8,128)(2,1)}, bf16[256,2048]{1,0:T(8,128)(2,1)S(1)}, u32[]{:S(2)}, u32[]{:S(2)}) %collective-permute-start.1) | collective-permute-done | bytes 1048608 | tf_op jit(solution)/shard_map/ppermute | solution.py:320
  172.6 46.1 %collective-permute-done.2 = bf16[256,2048]{1,0:T(8,128)(2,1)S(1)} collective-permute-done((bf16[256,2048]{1,0:T(8,128)(2,1)S(1)}, bf16[256,2048]{1,0:T(8,128)(2,1)S(1)}, u32[]{:S(2)}, u32[]{:S(2)}) %collective-permute-start.2) | collective-permute-done | bytes 1048608 | tf_op jit(solution)/shard_map/ppermute | solution.py:318
  218.7 3.2 %add_convert_fusion = bf16[256,2048]{1,0:T(8,128)(2,1)} fusion(bf16[256,2048]{1,0:T(8,128)(2,1)S(1)} %collective-permute-done.2, f32[256,2048]{1,0:T(8,128)} %get-tuple-element.34, bf16[256,2048]{1,0:T(8,128)(2,1)S(1)} %collective-permute-done.1, bf16[256,2048]{1,0:T(8,128)(2,1)S(1)} %get-tuple-element.21), kind=kLoop, calls=%fused_computation.1 | loop fusion | flops 3670016 | bytes 6291456 | tf_op jit(solution)/shard_map/convert_element_type | solution.py:321
  (17 shorter events, 0.0 us)
Async XLA Ops:
  2.8 2.5 %copy-start.11 = (bf16[1,2048,512]{2,1,0:T(8,128)(2,1)S(1)}, bf16[1,2048,512]{2,1,0:T(8,128)(2,1)}, u32[]{:S(2)}) copy-start(bf16[1,2048,512]{2,1,0:T(8,128)(2,1)} %param.26) | copy-start | bytes 6291460
  2.8 2.6 %copy-start.12 = (bf16[1,2048,512]{2,1,0:T(8,128)(2,1)S(1)}, bf16[1,2048,512]{2,1,0:T(8,128)(2,1)}, u32[]{:S(2)}) copy-start(bf16[1,2048,512]{2,1,0:T(8,128)(2,1)} %param.25) | copy-start | bytes 6291460
  5.4 0.7 copy-start.13
  6.1 1.6 copy-start.3
  6.1 1.6 copy-start
  6.1 1.6 copy-start.1
  6.1 1.8 copy-start.2
  6.2 1.8 copy-start.4
  133.2 1.0 copy-start.5
  134.2 1.0 copy-start.6
  135.2 1.0 copy-start.7
  136.1 0.6 copy-start.8
  136.7 0.6 copy-start.9
  137.3 0.6 copy-start.10
  151.5 2.9 %collective-permute-start = (bf16[256,2048]{1,0:T(8,128)(2,1)}, bf16[256,2048]{1,0:T(8,128)(2,1)S(1)}, u32[]{:S(2)}, u32[]{:S(2)}) collective-permute-start(bf16[256,2048]{1,0:T(8,128)(2,1)} %get-tuple-element.31), channel_id=1, source_target_pairs={{0,1},{1,0},{2,3},{3,2},{4,5},{5,4},{6,7},{7,6},{8,9},{9,8},{10,11... | collective-permute-start | bytes 3145736 | tf_op jit(solution)/shard_map/ppermute | solution.py:316
  169.7 2.9 %collective-permute-start.1 = (bf16[256,2048]{1,0:T(8,128)(2,1)}, bf16[256,2048]{1,0:T(8,128)(2,1)S(1)}, u32[]{:S(2)}, u32[]{:S(2)}) collective-permute-start(bf16[256,2048]{1,0:T(8,128)(2,1)} %get-tuple-element.35), channel_id=1, source_target_pairs={{0,1},{1,0},{2,3},{3,2},{4,5},{5,4},{6,7},{7,6},{8,9},{9,8},{10,11... | collective-permute-start | bytes 3145736 | tf_op jit(solution)/shard_map/ppermute | solution.py:320
  169.9 48.8 %collective-permute-start.2 = (bf16[256,2048]{1,0:T(8,128)(2,1)S(1)}, bf16[256,2048]{1,0:T(8,128)(2,1)S(1)}, u32[]{:S(2)}, u32[]{:S(2)}) collective-permute-start(bf16[256,2048]{1,0:T(8,128)(2,1)S(1)} %add_convert_fusion.1), channel_id=1, source_target_pairs={{0,16},{4,20},{8,24},{12,28},{16,0},{20,4},{24,8},{28,12},{1,17},{... | collective-permute-start | bytes 3145736 | tf_op jit(solution)/shard_map/ppermute | solution.py:318
